TPU v7x, 256 devices: a whole 4x4x8 slice. The times are simulated.
256 devices in a mesh: st: 64 (over z, x, core), tp: 4 (over y).
Axes of the slice: x: 4, y: 4, z: 8, core: 2. Of those that a mesh axis runs over, the one named last changes fastest.
Arguments:
- tokens: bfloat16 [65536, 4096], P('st'), may hold values from -6 to 6
- passage_ids: int32 [1024, 4], P('st'), may hold values from 0 to 191, as said below
- store: bfloat16 [192, 128, 4096], P('st'), may hold values from -6 to 6
- mix_gain: bfloat16 [4096], replicated, may hold values from 0.099609375 to 1.8984375
- w_query: bfloat16 [4096, 512], P(None, 'tp'), may hold values from -0.09375 to 0.09375
- w_key: bfloat16 [4096, 512], P(None, 'tp'), may hold values from -0.09375 to 0.09375
- w_value: bfloat16 [4096, 512], P(None, 'tp'), may hold values from -0.09375 to 0.09375
- w_cross_out: bfloat16 [512, 1024], P('tp'), may hold values from -0.5 to 0.5
- head_scale: float32 [4], replicated, may hold values from 1 to 4
- w_pool_in: bfloat16 [4096, 1024], P(None, 'tp'), may hold values from -0.09375 to 0.09375
- w_pool_mix: bfloat16 [4, 256, 256], replicated, may hold values from -0.375 to 0.375
- pool_scale: bfloat16 [1024], replicated, may hold values from 0.099609375 to 1.8984375
- gate_weight: float32 [1024], replicated, may hold values from -4 to 4
Outputs:
- mixed: bfloat16 [65536, 1024], P('st', 'tp')
Inputs may be any that keep to these rules, and one draw needn't show every extreme that they name: `passage_ids`: passage p is held by index p // 3 of st. The 64 ids of one index of st (its aligned blocks of rows) fall on exactly 32 owners, 2 ids on each; one owner receives 2 ids from every index of st.
All inputs are finite; a program needn't handle non-finite values.
Results may differ from a plain program's by a relative error of at most 0.013.
Values may be sent and summed in bfloat16 or wider, within the bound.
A program may use at most 128 MiB of HBM per device.

v0:
```python
import math

import jax
import jax.numpy as jnp
from jax import lax
from jax.sharding import PartitionSpec as P

HEAD_DIM = 128
GROUP_WIDTH = 256
SEQ_LEN = 128


EPSILON = 1e-06


def cut_along(x, dim, count):
    before, after = (x.shape[:dim], x.shape[dim + 1 :])
    return jnp.moveaxis(x.reshape(*before, count, -1, *after), dim, 0)


def summed_on_arrival(x, axis, dim):
    tiles = cut_along(x, dim, lax.axis_size(axis))
    arrived = lax.all_to_all(tiles, axis, split_axis=0, concat_axis=0, tiled=True)
    return arrived.astype(jnp.float32).sum(axis=0)


def head_normalize(values):
    return values * lax.rsqrt(jnp.mean(values * values, axis=-1, keepdims=True) + EPSILON)


def pool_residual(pooled_in, channel_ids):
    row_count, chan_width = pooled_in.shape
    sequences = pooled_in.astype(jnp.float32).reshape(row_count // SEQ_LEN, SEQ_LEN, chan_width)
    running = jnp.cumsum(sequences, axis=1)
    padded = jnp.concatenate(
        [jnp.zeros((sequences.shape[0], 16, chan_width), jnp.float32), running], axis=1
    )
    upper_sum = padded[:, 16:]
    position = jnp.arange(SEQ_LEN)[None, :, None]
    result = jnp.zeros_like(sequences)
    for section_index in range(4):
        window = 2 << section_index
        lower_sum = padded[:, 16 - window : 16 - window + SEQ_LEN]
        counted = jnp.minimum(position + 1, window).astype(jnp.float32)
        average = (upper_sum - lower_sum) / counted
        chosen = (channel_ids // GROUP_WIDTH == section_index)[None, None, :]
        result = jnp.where(chosen, average - sequences, result)
    return result.reshape(row_count, chan_width).astype(jnp.bfloat16)


def per_device(
    tokens,
    passage_ids,
    store,
    mix_gain,
    w_query,
    w_key,
    w_value,
    w_cross_out,
    head_scale,
    w_pool_in,
    w_pool_mix,
    pool_scale,
    gate_weight,
):
    row_count = tokens.shape[0]
    floats = tokens.astype(jnp.float32)
    scaled = floats * lax.rsqrt(jnp.mean(floats * floats, axis=-1, keepdims=True) + EPSILON)
    normed = (scaled * mix_gain.astype(jnp.float32)).astype(jnp.bfloat16)
    pooled_in = jnp.dot(normed, w_pool_in, preferred_element_type=jnp.float32).astype(jnp.bfloat16)
    local_width = pooled_in.shape[1]
    tensor_rank = lax.axis_index("tp")
    offset = tensor_rank * local_width
    residual = pool_residual(pooled_in, offset + jnp.arange(local_width))
    local_groups = local_width // GROUP_WIDTH
    mix_local = lax.dynamic_slice_in_dim(w_pool_mix, tensor_rank * local_groups, local_groups, 0)
    pool_out = jnp.einsum(
        "tgc,gce->tge",
        residual.reshape(row_count, local_groups, GROUP_WIDTH),
        mix_local,
        preferred_element_type=jnp.float32,
    )
    pool_out = pool_out.reshape(row_count, local_width) * lax.dynamic_slice_in_dim(
        pool_scale, offset, local_width
    ).astype(jnp.float32)
    gate_value = jax.nn.sigmoid(
        pooled_in.astype(jnp.float32) * lax.dynamic_slice_in_dim(gate_weight, offset, local_width)
    )
    heads_local = w_query.shape[1] // HEAD_DIM
    scales = lax.dynamic_slice_in_dim(
        head_scale, tensor_rank * heads_local, heads_local
    ) / math.sqrt(HEAD_DIM)
    queries = head_normalize(
        jnp.dot(normed, w_query, preferred_element_type=jnp.float32).reshape(
            row_count, heads_local, HEAD_DIM
        )
    ).astype(jnp.bfloat16)
    owned_count, passage_len = (store.shape[0], store.shape[1])
    flat_store = store.reshape(owned_count * passage_len, store.shape[2])
    keys_own = head_normalize(
        jnp.dot(flat_store, w_key, preferred_element_type=jnp.float32).reshape(
            owned_count, passage_len, heads_local, HEAD_DIM
        )
    ).astype(jnp.bfloat16)
    values_own = (
        jnp.dot(flat_store, w_value, preferred_element_type=jnp.float32)
        .astype(jnp.bfloat16)
        .reshape(owned_count, passage_len, heads_local, HEAD_DIM)
    )
    block_count, per_block = passage_ids.shape
    block_rows = row_count // block_count
    wanted = passage_ids.reshape(-1)
    request_count = wanted.shape[0]
    st_size = lax.axis_size("st")
    capacity = (2 * request_count + st_size - 1) // st_size
    owner_rank = wanted // owned_count
    local_index = wanted % owned_count
    onehot = (owner_rank[:, None] == jnp.arange(st_size)[None, :]).astype(jnp.int32)
    order_rank = jnp.sum((jnp.cumsum(onehot, axis=0) - onehot) * onehot, axis=1)
    slot_index = owner_rank * capacity + order_rank
    requests = (
        jnp.zeros((st_size * capacity,), jnp.int32)
        .at[slot_index]
        .set(local_index)
        .reshape(st_size, capacity)
    )
    block_queries = queries.reshape(block_count, block_rows, heads_local, HEAD_DIM)
    flat_queries = block_queries.reshape(block_count, block_rows, heads_local * HEAD_DIM)
    send_rows = flat_queries[jnp.arange(request_count) // per_block]
    query_buffer = (
        jnp.zeros((st_size * capacity, block_rows, heads_local * HEAD_DIM), jnp.bfloat16)
        .at[slot_index]
        .set(send_rows)
    )
    query_buffer = query_buffer.reshape(st_size, capacity, block_rows, heads_local * HEAD_DIM)
    got_queries, asked_for = (
        lax.all_to_all(query_buffer, "st", split_axis=0, concat_axis=0, tiled=True),
        lax.all_to_all(requests, "st", split_axis=0, concat_axis=0, tiled=True),
    )
    chosen_keys = keys_own[asked_for.reshape(-1)].reshape(
        st_size, capacity, passage_len, heads_local, HEAD_DIM
    )
    chosen_values = values_own[asked_for.reshape(-1)].reshape(
        st_size, capacity, passage_len, heads_local, HEAD_DIM
    )
    got_queries = got_queries.reshape(st_size, capacity, block_rows, heads_local, HEAD_DIM)
    scores = (
        jnp.einsum(
            "scqhd,sckhd->schqk", got_queries, chosen_keys, preferred_element_type=jnp.float32
        )
        * scales[None, None, :, None, None]
    )
    weights = jnp.exp(scores)
    part_totals = jnp.transpose(jnp.sum(weights, axis=4), (0, 1, 3, 2))
    partial_out = jnp.einsum(
        "schqk,sckhd->scqhd",
        weights.astype(jnp.bfloat16),
        chosen_values,
        preferred_element_type=jnp.float32,
    )
    partial_out = partial_out.astype(jnp.bfloat16).reshape(
        st_size, capacity, block_rows, heads_local * HEAD_DIM
    )
    back_out = lax.all_to_all(partial_out, "st", split_axis=0, concat_axis=0, tiled=True)
    back_totals = lax.all_to_all(
        part_totals.astype(jnp.bfloat16), "st", split_axis=0, concat_axis=0, tiled=True
    ).astype(part_totals.dtype)
    mine_out = back_out.reshape(st_size * capacity, block_rows, heads_local, HEAD_DIM)[
        slot_index
    ].astype(jnp.float32)
    summed = jnp.sum(
        mine_out.reshape(block_count, per_block, block_rows, heads_local, HEAD_DIM), axis=1
    )
    mine_totals = back_totals.reshape(st_size * capacity, block_rows, heads_local)[slot_index]
    totals = jnp.sum(mine_totals.reshape(block_count, per_block, block_rows, heads_local), axis=1)
    attended = (
        (summed / totals[..., None]).astype(jnp.bfloat16).reshape(row_count, heads_local * HEAD_DIM)
    )
    cross_term = jnp.dot(attended, w_cross_out, preferred_element_type=jnp.float32)
    cross_sum = summed_on_arrival(cross_term.astype(jnp.bfloat16), "tp", 1)
    return (pool_out + gate_value * cross_sum).astype(jnp.bfloat16)


def solution(mesh):
    return jax.shard_map(
        per_device,
        mesh=mesh,
        in_specs=(
            P("st", None),
            P("st", None),
            P("st", None, None),
            P(),
            P(None, "tp"),
            P(None, "tp"),
            P(None, "tp"),
            P("tp", None),
            P(),
            P(None, "tp"),
            P(),
            P(),
            P(),
        ),
        out_specs=P("st", "tp"),
        check_vma=False,
    )
```

profile of v0, /device:TPU:8, one launch (start us, length us, event | category | flops | bytes accessed | tf_op | source)
XLA Modules:
  0.0 227.6 jit_solution(1180496895974224864)
XLA Ops:
  0.0 0.0 copy-start
  0.0 0.8 broadcast_remainder_fusion
  0.8 0.8 compare_and_fusion
  1.7 0.1 copy.45
  1.7 0.1 div.130
  1.8 0.1 div.129
  1.9 0.1 copy.47
  2.0 0.1 rem.67
  2.1 0.1 copy.46
  2.2 0.1 ne.136
  2.3 0.1 fusion.46
  2.4 0.1 reduce_window_sum.23
  2.5 0.2 select_reduce_fusion
  2.7 0.1 copy.44
  2.8 0.1 and.78
  2.9 0.8 scatter_custom_fusion
  3.7 0.8 all_to_all.18
  4.4 11.9 %all-to-all-start = ((s32[64,1,2]{2,1,0:T(1,128)}), s32[64,1,2]{2,1,0:T(1,128)S(1)}, u32[]{:S(2)}, u32[]{:S(2)}) async-start(s32[64,1,2]{2,1,0:T(1,128)} %bitcast.10), calls=%async_computation | async-start | bytes 65536 | tf_op jit(solution)/shard_map/all_to_all | solution.py:138
  16.4 0.7 convert_element_type.142
  17.1 5.2 %fusion = f32[1024]{0:T(1024)S(1)} fusion(bf16[1024,4096]{1,0:T(8,128)(2,1)} %param.13), kind=kLoop, calls=%fused_computation.9 | loop fusion | flops 12581888 | bytes 8392704 | tf_op jit(solution)/shard_map/reduce_sum | solution.py:68
  22.3 0.5 copy-done.1
  22.9 3.8 %multiply_reduce_fusion = (f32[1024]{0:T(1024)S(1)}, f32[1024,128]{1,0:T(8,128)S(1)}) fusion(bf16[4096,128]{1,0:T(8,128)(2,1)} %param.17, bf16[1024,4096]{1,0:T(8,128)(2,1)S(1)} %copy-done.1, f32[4096]{0:T(1024)S(1)} %convert_element_type.142, f32[1024]{0:T(1024)S(1)} %add_rsqrt_fusion.1), kind=kOutput, calls=%fused_computation.56 | convolution fusion | flops 1090780160 | bytes 9986048 | tf_op jit(solution)/shard_map/dot_general | solution.py:94
  26.6 0.2 multiply_convert_fusion
  26.8 1.7 gather_fusion.1
  28.5 1.9 broadcast_in_dim.57
  30.4 9.1 %scatter_fusion = bf16[128,64,128]{2,1,0:T(8,128)(2,1)} fusion(bf16[128,64,128]{2,1,0:T(8,128)(2,1)} %broadcast_in_dim.57, s32[64]{0:T(128)S(1)} %fusion.50, bf16[64,64,128]{2,1,0:T(8,128)(2,1)} %gather_fusion.1), kind=kCustom, calls=%fused_computation.6 | custom fusion | bytes 3145984 | tf_op jit(solution)/shard_map/scatter | solution.py:133
  39.5 0.0 all-to-all-done
  39.5 10.7 %all-to-all-start.1 = ((bf16[64,2,64,128]{3,2,1,0:T(8,128)(2,1)}), bf16[64,2,64,128]{3,2,1,0:T(8,128)(2,1)}, u32[]{:S(2)}, u32[]{:S(2)}) async-start(bf16[64,2,64,128]{3,2,1,0:T(8,128)(2,1)} %bitcast.80), calls=%async_computation.1 | async-start | bytes 4194304 | tf_op jit(solution)/shard_map/all_to_all | solution.py:137
  50.2 0.0 copy-done.4
  50.2 0.0 copy-start.2
  50.2 0.6 dynamic_slice.15
  51.5 0.0 copy-done
  51.5 2.3 %multiply_reduce_fusion.1 = (f32[384]{0:T(512)S(1)}, f32[384,128]{1,0:T(8,128)S(1)}) fusion(bf16[384,4096]{1,0:T(8,128)(2,1)S(1)} %bitcast.76, bf16[4096,128]{1,0:T(8,128)(2,1)} %param.18), kind=kOutput, calls=%fused_computation.58 | convolution fusion | flops 402751104 | bytes 4392448 | tf_op jit(solution)/shard_map/dot_general | solution.py:101
  53.8 0.1 fusion.45
  53.9 1.0 convolution_convert_fusion.1
  54.9 0.5 broadcast.459
  55.4 0.7 reduce.11
  56.2 0.1 reshape.405
  56.3 3.1 %gather_fusion.2 = bf16[128,128,128]{2,1,0:T(8,128)(2,1)} fusion(bf16[3,128,128]{2,1,0:T(8,128)(2,1)S(1)} %fusion.45, s32[1024]{0:T(1024)S(1)} %pad_clamp_fusion.1), kind=kCustom, calls=%fused_computation.2 | custom fusion | bytes 8389120 | tf_op jit(solution)/shard_map/gather | solution.py:140
  59.4 3.0 %gather_fusion = bf16[128,128,128]{2,1,0:T(8,128)(2,1)} fusion(bf16[3,128,128]{2,1,0:T(8,128)(2,1)S(1)} %bitcast.77, s32[1024]{0:T(1024)S(1)} %pad_clamp_fusion.1), kind=kCustom, calls=%fused_computation | custom fusion | bytes 8389120 | tf_op jit(solution)/shard_map/gather | solution.py:143
  62.4 38.8 %all-to-all-done.1 = bf16[64,2,64,128]{3,2,1,0:T(8,128)(2,1)} async-done(((bf16[64,2,64,128]{3,2,1,0:T(8,128)(2,1)}), bf16[64,2,64,128]{3,2,1,0:T(8,128)(2,1)}, u32[]{:S(2)}, u32[]{:S(2)}) %all-to-all-start.1) | async-done | bytes 2097184 | tf_op jit(solution)/shard_map/all_to_all | solution.py:137
  101.2 8.4 %fusion.3 = (bf16[64,2,64]{2,1,0:T(2,128)(2,1)}, f32[64,2,64,128]{3,2,1,0:T(8,128)}) fusion(f32[]{:T(128)} %bitcast.20, bf16[64,2,64,128]{3,2,1,0:T(8,128)(2,1)} %all-to-all-done.1, bf16[64,2,128,128]{3,2,1,0:T(8,128)(2,1)} %bitcast.79), kind=kOutput, calls=%fused_computation.14 | convolution fusion | flops 270524416 | bytes 10502148 | tf_op jit(solution)/shard_map/scqhd,sckhd->schqk/dot_general | solution.py:148
  109.6 5.3 %all-to-all-start.3 = ((bf16[64,2,64,1]{2,1,3,0:T(2,128)(2,1)}), bf16[64,2,64,1]{2,1,3,0:T(2,128)(2,1)S(1)}, u32[]{:S(2)}, u32[]{:S(2)}) async-start(bf16[64,2,64,1]{2,1,3,0:T(2,128)(2,1)} %bitcast.62), calls=%async_computation.3 | async-start | bytes 65536 | tf_op jit(solution)/shard_map/all_to_all | solution.py:165
  115.0 6.1 %convert_bitcast_fusion = bf16[64,2,64,128]{3,2,1,0:T(8,128)(2,1)} fusion(bf16[64,2,128,128]{3,2,1,0:T(8,128)(2,1)} %bitcast.78, f32[64,2,64,128]{3,2,1,0:T(8,128)} %get-tuple-element.16, f32[]{:T(128)} %bitcast.20), kind=kOutput, calls=%fused_computation.20 | convolution fusion | flops 271581184 | bytes 10485764 | tf_op jit(solution)/shard_map/schqk,sckhd->scqhd/dot_general | solution.py:155
  121.1 3.5 %all-to-all-done.3 = bf16[64,2,64,1]{2,1,3,0:T(2,128)(2,1)S(1)} async-done(((bf16[64,2,64,1]{2,1,3,0:T(2,128)(2,1)}), bf16[64,2,64,1]{2,1,3,0:T(2,128)(2,1)S(1)}, u32[]{:S(2)}, u32[]{:S(2)}) %all-to-all-start.3) | async-done | bytes 16416 | tf_op jit(solution)/shard_map/all_to_all | solution.py:165
  124.5 7.2 %all-to-all-start.2 = ((bf16[64,2,64,128]{3,2,1,0:T(8,128)(2,1)}), bf16[64,2,64,128]{3,2,1,0:T(8,128)(2,1)}, u32[]{:S(2)}, u32[]{:S(2)}) async-start(bf16[64,2,64,128]{3,2,1,0:T(8,128)(2,1)} %convert_bitcast_fusion), calls=%async_computation.2 | async-start | bytes 4194304 | tf_op jit(solution)/shard_map/all_to_all | solution.py:164
  131.8 0.6 gather_fusion.4
  132.4 0.1 div.137
  132.5 50.4 %all-to-all-done.2 = bf16[64,2,64,128]{3,2,1,0:T(8,128)(2,1)} async-done(((bf16[64,2,64,128]{3,2,1,0:T(8,128)(2,1)}), bf16[64,2,64,128]{3,2,1,0:T(8,128)(2,1)}, u32[]{:S(2)}, u32[]{:S(2)}) %all-to-all-start.2) | async-done | bytes 2097184 | tf_op jit(solution)/shard_map/all_to_all | solution.py:164
  183.0 3.3 %gather_fusion.3 = bf16[64,64,128]{2,1,0:T(8,128)(2,1)} fusion(bf16[128,64,128]{2,1,0:T(8,128)(2,1)} %bitcast.24, s32[1024]{0:T(1024)S(1)} %pad_clamp_fusion), kind=kCustom, calls=%fused_computation.3 | custom fusion | bytes 2097408 | tf_op jit(solution)/shard_map/gather | solution.py:168
  186.2 1.5 convert_reduce_fusion.1
  187.7 0.2 fusion.42
  187.9 2.1 convolution_convert_fusion
  190.0 4.9 %all-to-all-start.4 = ((bf16[4,1024,256]{1,2,0:T(8,128)(2,1)}), bf16[4,1024,256]{1,2,0:T(8,128)(2,1)}, u32[]{:S(2)}, u32[]{:S(2)}) async-start(bf16[4,1024,256]{1,2,0:T(8,128)(2,1)} %bitcast.81), calls=%async_computation.4 | async-start | bytes 4194304 | tf_op jit(solution)/shard_map/all_to_all | solution.py:23
  194.9 7.3 %fusion.20 = f32[1024,256]{1,0:T(8,128)} fusion(bf16[4096,256]{1,0:T(8,128)(2,1)} %param.22, bf16[1024,4096]{1,0:T(8,128)(2,1)} %param.13, f32[4096]{0:T(1024)S(1)} %convert_element_type.142, f32[1024]{0:T(1024)S(1)} %add_rsqrt_fusion.1), kind=kOutput, calls=%fused_computation.28 | convolution fusion | flops 2164785152 | bytes 11554816 | tf_op jit(solution)/shard_map/dot_general | solution.py:70
  202.3 1.8 fusion.40
  204.1 3.1 %fusion.39 = bf16[8,128,256]{2,0,1:T(8,128)(2,1)S(1)} fusion(f32[8,128,256]{2,0,1:T(8,128)S(1)} %fusion.40, f32[8,128,256]{2,1,0:T(8,128)} %bitcast.84, f32[128]{0:T(128)S(1)} %get-tuple-element.21, f32[128]{0:T(128)S(1)} %get-tuple-element.22, f32[128]{0:T(128)S(1)} %get-tuple-element.23, f32[128]{0:T(128)S(1)} %get-tuple-element.24, ...), kind=kLoop, calls=%fused_computation.50 | loop fusion | flops 4456448 | bytes 2624512 | tf_op jit(solution)/shard_map/convert_element_type | solution.py:48
  207.3 0.9 copy.42
  208.2 0.8 dynamic_slice.14
  208.9 0.8 dynamic-slice_convert_fusion
  209.7 9.3 %all-to-all-done.4 = bf16[4,1024,256]{1,2,0:T(8,128)(2,1)} async-done(((bf16[4,1024,256]{1,2,0:T(8,128)(2,1)}), bf16[4,1024,256]{1,2,0:T(8,128)(2,1)}, u32[]{:S(2)}, u32[]{:S(2)}) %all-to-all-start.4) | async-done | bytes 2097184 | tf_op jit(solution)/shard_map/all_to_all | solution.py:23
  219.0 3.1 %convert_reduce_fusion = f32[1024,256]{0,1:T(8,128)} fusion(bf16[4,1024,256]{1,2,0:T(8,128)(2,1)} %all-to-all-done.4), kind=kLoop, calls=%fused_computation.12 | loop fusion | flops 1835008 | bytes 3145728 | tf_op jit(solution)/shard_map/reduce_sum | solution.py:24
  222.0 2.5 %copy.50 = f32[1024,256]{1,0:T(8,128)} copy(f32[1024,256]{0,1:T(8,128)} %convert_reduce_fusion) | data formatting | bytes 2097152 | tf_op jit(solution)/shard_map/reduce_sum | solution.py:24
  224.6 3.0 %fusion.16 = bf16[1024,256]{1,0:T(8,128)(2,1)} fusion(bf16[1024,256]{1,0:T(8,128)(2,1)} %bitcast.86, f32[1024,256]{1,0:T(8,128)} %copy.50, f32[1024,256]{1,0:T(8,128)} %fusion.20, f32[256]{0:T(256)S(1)} %dynamic_slice.14, f32[256]{0:T(256)S(1)} %dynamic-slice_convert_fusion, bf16[4,256,256]{2,1,0:T(8,128)(2,1)} %param.23, s32[]{:T(128)S(6)} %select_n.110), kind=kOutput, calls=%fused_computation.26 | convolution fusion | flops 136314880 | bytes 3278852 | tf_op jit(solution)/shard_map/tgc,gce->tge/dot_general | solution.py:77
  (21 shorter events, 0.2 us)
Async XLA Ops:
  0.0 51.5 %copy-start = (bf16[3,128,4096]{2,1,0:T(8,128)(2,1)S(1)}, bf16[3,128,4096]{2,1,0:T(8,128)(2,1)}, u32[]{:S(2)}) copy-start(bf16[3,128,4096]{2,1,0:T(8,128)(2,1)} %param.15) | copy-start | bytes 9437188
  4.4 35.0 %all-to-all-start = ((s32[64,1,2]{2,1,0:T(1,128)}), s32[64,1,2]{2,1,0:T(1,128)S(1)}, u32[]{:S(2)}, u32[]{:S(2)}) async-start(s32[64,1,2]{2,1,0:T(1,128)} %bitcast.10), calls=%async_computation | async-start | bytes 65536 | tf_op jit(solution)/shard_map/all_to_all | solution.py:138
  17.1 5.8 %copy-start.1 = (bf16[1024,4096]{1,0:T(8,128)(2,1)S(1)}, bf16[1024,4096]{1,0:T(8,128)(2,1)}, u32[]{:S(2)}) copy-start(bf16[1024,4096]{1,0:T(8,128)(2,1)} %param.13) | copy-start | bytes 25165828
  30.4 19.9 %copy-start.4 = (f32[4]{0:T(128)S(1)}, f32[4]{0:T(128)}, u32[]{:S(2)}) copy-start(f32[4]{0:T(128)} %param.21) | copy-start | bytes 52
  39.5 61.7 %all-to-all-start.1 = ((bf16[64,2,64,128]{3,2,1,0:T(8,128)(2,1)}), bf16[64,2,64,128]{3,2,1,0:T(8,128)(2,1)}, u32[]{:S(2)}, u32[]{:S(2)}) async-start(bf16[64,2,64,128]{3,2,1,0:T(8,128)(2,1)} %bitcast.80), calls=%async_computation.1 | async-start | bytes 4194304 | tf_op jit(solution)/shard_map/all_to_all | solution.py:137
  50.2 3.7 %copy-start.2 = (bf16[4096,128]{1,0:T(8,128)(2,1)S(1)}, bf16[4096,128]{1,0:T(8,128)(2,1)}, u32[]{:S(2)}) copy-start(bf16[4096,128]{1,0:T(8,128)(2,1)} %param.19) | copy-start | bytes 3145732
  109.6 14.9 %all-to-all-start.3 = ((bf16[64,2,64,1]{2,1,3,0:T(2,128)(2,1)}), bf16[64,2,64,1]{2,1,3,0:T(2,128)(2,1)S(1)}, u32[]{:S(2)}, u32[]{:S(2)}) async-start(bf16[64,2,64,1]{2,1,3,0:T(2,128)(2,1)} %bitcast.62), calls=%async_computation.3 | async-start | bytes 65536 | tf_op jit(solution)/shard_map/all_to_all | solution.py:165
  121.1 66.8 %copy-start.3 = (bf16[128,1024]{1,0:T(8,128)(2,1)S(1)}, bf16[128,1024]{1,0:T(8,128)(2,1)}, u32[]{:S(2)}) copy-start(bf16[128,1024]{1,0:T(8,128)(2,1)} %param.20) | copy-start | bytes 786436
  124.5 58.4 %all-to-all-start.2 = ((bf16[64,2,64,128]{3,2,1,0:T(8,128)(2,1)}), bf16[64,2,64,128]{3,2,1,0:T(8,128)(2,1)}, u32[]{:S(2)}, u32[]{:S(2)}) async-start(bf16[64,2,64,128]{3,2,1,0:T(8,128)(2,1)} %convert_bitcast_fusion), calls=%async_computation.2 | async-start | bytes 4194304 | tf_op jit(solution)/shard_map/all_to_all | solution.py:164
  190.0 29.0 %all-to-all-start.4 = ((bf16[4,1024,256]{1,2,0:T(8,128)(2,1)}), bf16[4,1024,256]{1,2,0:T(8,128)(2,1)}, u32[]{:S(2)}, u32[]{:S(2)}) async-start(bf16[4,1024,256]{1,2,0:T(8,128)(2,1)} %bitcast.81), calls=%async_computation.4 | async-start | bytes 4194304 | tf_op jit(solution)/shard_map/all_to_all | solution.py:23
where the time goes:
time: 230 us; the launch traced here: 228 us
  waiting for transfers between devices  102 us (44%)
  starting transfers between devices  40.2 us (17%)
  matrix products  33.9 us (15%)
  local copies, waits for them, and re-layouts  31 us (13%)
  other arithmetic  19.6 us (9%)
    all_to_all x1, waiting for transfers between devices, per_device(): lax.all_to_all(partial_out, 'st', split_axis=0, concat_axis=0, tiled=True)  50.4 us
    all_to_all x1, waiting for transfers between devices, per_device(): lax.all_to_all(query_buffer, 'st', split_axis=0, concat_axis=0, tiled=True)  38.8 us
    all_to_all x1, starting transfers between devices, per_device(): lax.all_to_all(requests, 'st', split_axis=0, concat_axis=0, tiled=True)  11.9 us
    all_to_all x1, starting transfers between devices, per_device(): lax.all_to_all(query_buffer, 'st', split_axis=0, concat_axis=0, tiled=True)  10.7 us
    all_to_all x1, waiting for transfers between devices, summed_on_arrival(): lax.all_to_all(tiles, axis, split_axis=0, concat_axis=0, tiled=True)  9.3 us
    scatter x1, local copies, waits for them, and re-layouts, per_device(): query_buffer = jnp.zeros((st_size * capacity, block_rows, heads_local * H...  9.1 us
    dot_general x1, matrix products, per_device(): jnp.einsum('scqhd,sckhd->schqk', got_queries, chosen_keys, preferred_elem...  8.43 us
    dot_general x1, matrix products, per_device(): jnp.dot(normed, w_pool_in, preferred_element_type=jnp.float32)  7.34 us
  transfers between devices with their start and end apart: 5, of which 4 were waited for; matrix products, arithmetic and copies ran while one was open for 24% of the time, Pallas kernels for 0%

commit v1 on v0

v1 whole, which is shorter than its diff:
```python
import functools
import math

import jax
import jax.numpy as jnp
from jax import lax
from jax.experimental import pallas as pl
from jax.experimental.pallas import tpu as pltpu
from jax.sharding import PartitionSpec as P

MESH = pl.DeviceIdType.MESH
BF = jnp.bfloat16
F32 = jnp.float32

EPSILON = 1e-06
NZ, NX, NC, NY = 8, 4, 2, 4
D = 4096
HD = 128
GW = 256
ROWS = 1024
BLOCK = 64
NPB = 4
NBLK = 16
PLEN = 128
OWN = 3
SEQ = 128
SLOTS = NZ * NC * OWN
TCHUNK = 256
QTR = 256


def kernel(
    tok_h, ids_h, store_h, gain_h, wq_h, wk_h, wv_h, wc_h, hs_s, wp_h, wm_h, ps_h, gw_h,
    out_h,
    tok_v, store_v, wkv_v, wq_v, wp_v, wm_v, gain_v, ps_v, gw_v,
    kt_v, v_v, qg_v, idv, ids_s, wc_v,
    pooled_v, pool_v, gate_v, e_v, part_v, rly_v, sum_v, rrecv_v, tot_v, totg_v, att_v, out_v,
    lsem, tsem, osem,
    zs, zr, cs, cr, qs, qr, ids_ss, ids_rs, wcs, wcr, ts, tr, rs, rr, ys, yr,
):
    s = lax.axis_index("st")
    y = lax.axis_index("tp")
    c = lax.rem(s, NC)
    x = lax.rem(lax.div(s, NC), NX)
    z = lax.div(s, NC * NX)

    def dev(dz=0, dx=0, dy=0, other=False):
        cc = 1 - c if other else c
        zz = lax.rem(z + dz + NZ, NZ)
        xx = lax.rem(x + dx + NX, NX)
        yy = lax.rem(y + dy + NY, NY)
        return (zz * (NX * NC) + xx * NC + cc, yy)

    def remote(src, dst, ssem, rsem, to):
        return pltpu.make_async_remote_copy(
            src_ref=src, dst_ref=dst, send_sem=ssem, recv_sem=rsem,
            device_id=to, device_id_type=MESH,
        )

    barrier = pltpu.get_barrier_semaphore()
    partners = [
        dev(dz=1), dev(dz=-1), dev(dx=1), dev(dx=-1), dev(dx=2),
        dev(dy=1), dev(dy=-1), dev(dy=2), dev(other=True),
    ]
    for to in partners:
        pl.semaphore_signal(barrier, inc=1, device_id=to, device_id_type=MESH)

    def local(src, dst, sem):
        copy = pltpu.make_async_copy(src, dst, sem)
        copy.start()
        return copy

    kv_loads = [
        local(wk_h, wkv_v.at[:, pl.ds(0, HD)], lsem.at[0]),
        local(wv_h, wkv_v.at[:, pl.ds(HD, HD)], lsem.at[1]),
        local(store_h, store_v, lsem.at[2]),
    ]
    gain_load = local(gain_h, gain_v, lsem.at[3])
    wq_load = local(wq_h, wq_v, lsem.at[4])
    tok_loads = [
        local(
            tok_h.at[pl.ds(i * TCHUNK, TCHUNK)], tok_v.at[pl.ds(i * TCHUNK, TCHUNK)], tsem.at[i]
        )
        for i in range(ROWS // TCHUNK)
    ]
    wp_load = local(wp_h, wp_v, lsem.at[5])
    pool_loads = [
        local(wm_h.at[y], wm_v, lsem.at[6]),
        local(ps_h, ps_v, lsem.at[7]),
        local(gw_h, gw_v, lsem.at[8]),
    ]
    ids_own = local(ids_h, idv.at[0], lsem.at[9])
    wc_own = local(
        wc_h.at[:, pl.ds(pl.multiple_of(y * GW, GW), GW)], wc_v.at[y], lsem.at[10]
    )

    pl.semaphore_wait(barrier, len(partners))

    sends = []

    for r in (1, 2, 3):
        cp = remote(ids_h, idv.at[NX - r], ids_ss.at[r], ids_rs.at[NX - r], dev(dx=r))
        cp.start()
        sends.append(cp)
    for r in (1, 2, 3):
        column = pl.multiple_of(lax.rem(y + r, NY) * GW, GW)
        cp = remote(
            wc_h.at[:, pl.ds(column, GW)], wc_v.at[y], wcs.at[r], wcr.at[NY - r], dev(dy=r)
        )
        cp.start()
        sends.append(cp)

    for load in kv_loads:
        load.wait()
    kv = jnp.dot(store_v[...].reshape(OWN * PLEN, D), wkv_v[...], preferred_element_type=F32)
    keys = kv[:, :HD]
    keys = keys * lax.rsqrt(jnp.mean(keys * keys, axis=-1, keepdims=True) + EPSILON)
    own_slot = (z * NC + c) * OWN
    for i in range(OWN):
        rows = slice(i * PLEN, (i + 1) * PLEN)
        kt_v[own_slot + i] = jnp.transpose(keys[rows]).astype(BF)
        v_v[own_slot + i] = kv[rows, HD:].astype(BF)

    bufs = (kt_v, v_v)

    def group(kind, origin, core):
        return bufs[kind].at[pl.ds((origin * NC + core) * OWN, OWN)]

    def z_copy(d, kind, k, to_next):
        sign = 1 if d == 0 else -1
        back = k if to_next else k + 1
        origin = lax.rem(z - sign * back + NZ, NZ)
        block = group(kind, origin, c)
        i = d * 8 + kind * 4 + k
        return remote(block, block, zs.at[i], zr.at[i], dev(dz=sign))

    def z_send(d, kind, k):
        cp = z_copy(d, kind, k, True)
        cp.start()
        sends.append(cp)

    def core_send(kind, o):
        block = group(kind, lax.rem(z + o, NZ), c)
        i = kind * NZ + o
        cp = remote(block, block, cs.at[i], cr.at[i], dev(other=True))
        cp.start()
        sends.append(cp)

    def core_wait(kind, o):
        block = group(kind, lax.rem(z + o, NZ), 1 - c)
        i = kind * NZ + o
        remote(block, block, cs.at[i], cr.at[i], dev(other=True)).wait_recv()

    def z_advance(d, kind, k):
        z_copy(d, kind, k, False).wait_recv()
        if k < 2 or (k == 2 and kind == d):
            z_send(d, kind, k + 1)
        back = k + 1
        core_send(kind, back if d == 1 else NZ - back)

    for kind in (0, 1):
        for d in (0, 1):
            z_send(d, kind, 0)
    for kind in (0, 1):
        core_send(kind, 0)

    gain_load.wait()
    wq_load.wait()
    gain = gain_v[...]

    def q_copy(d, m, sending):
        sign = 1 if d == 0 else -1
        if m < 2:
            half, back = m, 0
        else:
            half, back = d, 1
        origin = back if sending else back + 1
        row = (origin if d == 1 else NX - origin) % NX
        at = qg_v.at[row, pl.ds(half * (ROWS // 2), ROWS // 2)]
        back_there = back + 1
        row_there = (back_there if d == 1 else NX - back_there) % NX
        to = qg_v.at[row_there, pl.ds(half * (ROWS // 2), ROWS // 2)] if sending else at
        i = d * 3 + m
        return remote(at, to, qs.at[i], qr.at[i], dev(dx=sign))

    def q_send(d, m):
        cp = q_copy(d, m, True)
        cp.start()
        sends.append(cp)

    scales = []

    def query_chunk(i):
        tok_loads[i].wait()
        t = tok_v[pl.ds(i * TCHUNK, TCHUNK), :]
        tf = t.astype(F32)
        scale = lax.rsqrt(jnp.mean(tf * tf, axis=-1, keepdims=True) + EPSILON)
        scales.append(scale)
        tg = t * gain
        tok_v[pl.ds(i * TCHUNK, TCHUNK), :] = tg
        q = jnp.dot(tg, wq_v[...], preferred_element_type=F32) * scale
        q = q * lax.rsqrt(jnp.mean(q * q, axis=-1, keepdims=True) + EPSILON)
        qg_v[0, pl.ds(i * TCHUNK, TCHUNK), :] = q.astype(BF)

    per_half = ROWS // 2 // TCHUNK
    for half in (0, 1):
        for i in range(per_half):
            query_chunk(half * per_half + i)
        for d in (0, 1):
            q_send(d, half)

    for kind in (0, 1):
        for d in (0, 1):
            z_advance(d, kind, 0)

    wp_load.wait()
    for i in range(ROWS // TCHUNK):
        tg = tok_v[pl.ds(i * TCHUNK, TCHUNK), :]
        pooled = jnp.dot(tg, wp_v[...], preferred_element_type=F32) * scales[i]
        pooled_v[pl.ds(i * TCHUNK, TCHUNK), :] = pooled.astype(BF)

    for d in (0, 1):
        z_advance(d, 0, 1)

    for d in (0, 1):
        q_copy(d, d, False).wait_recv()
        q_send(d, 2)

    for load in pool_loads:
        load.wait()
    window = lax.shift_left(jnp.int32(2), y.astype(jnp.int32))
    row_id = lax.broadcasted_iota(jnp.int32, (SEQ, SEQ), 0)
    col_id = lax.broadcasted_iota(jnp.int32, (SEQ, SEQ), 1)
    band = jnp.where((col_id <= row_id) & (col_id > row_id - window), 1.0, 0.0).astype(BF)
    position = lax.broadcasted_iota(jnp.int32, (SEQ, GW), 0)
    inverse = 1.0 / jnp.minimum(position + 1, window).astype(F32)
    ps_all = ps_v[...].astype(F32)
    gw_all = gw_v[...]
    ps = jnp.zeros((1, GW), F32)
    gw = jnp.zeros((1, GW), F32)
    for g in range(NY):
        here = y == g
        ps = ps + jnp.where(here, ps_all[g : g + 1], 0.0)
        gw = gw + jnp.where(here, gw_all[g : g + 1], 0.0)

    def pool_body(i, carry):
        rows = pl.ds(pl.multiple_of(i * SEQ, SEQ), SEQ)
        p = pooled_v[rows, :]
        pf = p.astype(F32)
        sums = jnp.dot(band, p, preferred_element_type=F32)
        residual = (sums * inverse - pf).astype(BF)
        pool_v[rows, :] = jnp.dot(residual, wm_v[...], preferred_element_type=F32) * ps
        gate_v[rows, :] = 1.0 / (1.0 + jnp.exp(-(pf * gw)))
        return carry

    lax.fori_loop(0, ROWS // SEQ, pool_body, 0)

    for d in (0, 1):
        z_advance(d, 1, 1)

    ids_own.wait()
    for r in (1, 2, 3):
        remote(ids_h, idv.at[r], ids_ss.at[r], ids_rs.at[r], dev(dx=r)).wait_recv()
    ids_load = local(idv, ids_s, lsem.at[11])
    ids_load.wait()

    for d in (0, 1):
        q_copy(d, 1 - d, False).wait_recv()
    for d in (0, 1):
        z_advance(d, 0, 2)
    for d in (0, 1):
        z_advance(d, 1, 2)
    for d in (0, 1):
        q_copy(d, 2, False).wait_recv()
    for o in range(NZ):
        if o != 4:
            core_wait(0, o)
    z_advance(0, 0, 3)
    core_wait(0, 4)

    scale = hs_s[y] * (1.0 / math.sqrt(HD))
    eye = row_id == col_id

    def slot_of(r, b, j):
        p = ids_s[r, b, j]
        owner = lax.div(p, OWN)
        zo = lax.div(owner, NX * NC)
        xo = lax.rem(lax.div(owner, NC), NX)
        co = lax.rem(owner, NC)
        return (zo * NC + co) * OWN + lax.rem(p, OWN), xo == x

    def score_pair(r, pair):
        totals = []
        for u in (0, 1):
            b = pair * 2 + u
            q = qg_v[r, pl.ds(pl.multiple_of(b * BLOCK, BLOCK), BLOCK), :]
            found = [slot_of(r, b, j) for j in range(NPB)]
            kt = jnp.concatenate([kt_v[slot] for slot, _ in found], axis=1)
            sc = jnp.dot(q, kt, preferred_element_type=F32)
            e = jnp.exp(sc * scale)
            es = [
                jnp.where(found[j][1], e[:, j * PLEN : (j + 1) * PLEN], 0.0) for j in range(NPB)
            ]
            at = pl.multiple_of(b * BLOCK, BLOCK)
            for j in range(NPB):
                e_v[r, pl.ds(at, BLOCK), pl.ds(j * PLEN, PLEN)] = es[j].astype(BF)
            both = (es[0] + es[1]) + (es[2] + es[3])
            totals.append(jnp.sum(both, axis=1, keepdims=True))
        column = jnp.concatenate(totals, axis=0)
        row = jnp.sum(jnp.where(eye, column, 0.0), axis=0, keepdims=True)
        tot_v[r, pl.ds(pair, 1), :] = row

    for r in (2, 1, 3, 0):

        def score_body(i, carry, r=r):
            score_pair(r, i * 2)
            score_pair(r, i * 2 + 1)
            return carry

        lax.fori_loop(0, NBLK // 4, score_body, 0)
        if r:
            cp = remote(tot_v.at[r], totg_v.at[NX - r], ts.at[r], tr.at[NX - r], dev(dx=r))
            cp.start()
            sends.append(cp)

    for o in range(NZ):
        if o != 4:
            core_wait(1, o)
    z_advance(1, 1, 3)
    core_wait(1, 4)

    def value_quarter(r, quarter):
        def body(i, carry):
            for u in (0, 1):
                b = quarter * 4 + i * 2 + u
                at = pl.multiple_of(b * BLOCK, BLOCK)
                vv = jnp.concatenate([v_v[slot_of(r, b, j)[0]] for j in range(NPB)], axis=0)
                o = jnp.dot(e_v[r, pl.ds(at, BLOCK), :], vv, preferred_element_type=F32)
                part_v[r, pl.ds(at, BLOCK), :] = o.astype(BF)
            return carry

        lax.fori_loop(0, 2, body, 0)

    def rows_of(quarter):
        return pl.ds(quarter * QTR, QTR)

    def r_copy(d, m, src, dst):
        i = d * 6 + m
        return remote(src, dst, rs.at[i], rr.at[i], dev(dx=1 if d == 0 else -1))

    def r_send(d, m, src, dst):
        cp = r_copy(d, m, src, dst)
        cp.start()
        sends.append(cp)

    for step in (0, 1):
        for d in (0, 1):
            quarter = 2 * d + step
            value_quarter(2, quarter)
            r_send(
                d, step, part_v.at[2, rows_of(quarter)], rly_v.at[d, pl.ds(step * QTR, QTR)]
            )
    near = (1, 3)
    for step in (0, 1):
        for d in (0, 1):
            quarter = 2 * (1 - d) + step
            value_quarter(near[d], quarter)
            r_send(
                d, 2 + step, part_v.at[near[d], rows_of(quarter)], rrecv_v.at[d, rows_of(quarter)]
            )
    for step in (0, 1):
        for d in (0, 1):
            value_quarter(near[d], 2 * d + step)
    for step in (0, 1):
        for d in (0, 1):
            quarter = 2 * d + step
            here = pl.ds(step * QTR, QTR)
            r_copy(d, step, part_v.at[2, rows_of(quarter)], rly_v.at[d, here]).wait_recv()
            both = rly_v[d, here, :].astype(F32) + part_v[near[d], rows_of(quarter), :].astype(F32)
            sum_v[d, here, :] = both.astype(BF)
            r_send(d, 4 + step, sum_v.at[d, here], rrecv_v.at[d, rows_of(quarter)])
    for quarter in range(4):
        value_quarter(0, quarter)

    for r in (1, 2, 3):
        remote(tot_v.at[r], totg_v.at[r], ts.at[r], tr.at[r], dev(dx=r)).wait_recv()
    all_totals = tot_v[0] + totg_v[1] + totg_v[2] + totg_v[3]

    def y_copy(d, m, quarter, sending):
        sign = 1 if d == 0 else -1
        back = (0 if m < 4 else 1) + (0 if sending else 1)
        head = lax.rem(y - sign * back + NY, NY)
        block = att_v.at[head, rows_of(quarter)]
        i = d * 6 + m
        return remote(block, block, ys.at[i], yr.at[i], dev(dy=sign))

    order = (0, 2, 1, 3)
    for n, quarter in enumerate(order):
        step = quarter % 2
        for d in (0, 1):
            m = (4 + step) if d == quarter // 2 else (2 + step)
            r_copy(d, m, rrecv_v.at[d, rows_of(quarter)], rrecv_v.at[d, rows_of(quarter)]).wait_recv()
        columns = []
        for pair in range(2):
            row = all_totals[quarter * 2 + pair : quarter * 2 + pair + 1, :]
            columns.append(jnp.sum(jnp.where(eye, row, 0.0), axis=1, keepdims=True))
        total = jnp.concatenate(columns, axis=0)
        summed = (
            part_v[0, rows_of(quarter), :].astype(F32)
            + rrecv_v[0, rows_of(quarter), :].astype(F32)
            + rrecv_v[1, rows_of(quarter), :].astype(F32)
        )
        att_v[y, rows_of(quarter), :] = (summed * (1.0 / total)).astype(BF)
        for d in (0, 1):
            cp = y_copy(d, n, quarter, True)
            cp.start()
            sends.append(cp)

    for n, quarter in enumerate(order):
        d = quarter // 2
        y_copy(d, n, quarter, False).wait_recv()
        cp = y_copy(d, 4 + quarter % 2, quarter, True)
        cp.start()
        sends.append(cp)

    wc_own.wait()
    for r in (1, 2, 3):
        remote(
            wc_h.at[:, pl.ds(0, GW)], wc_v.at[lax.rem(y + r, NY)], wcs.at[r], wcr.at[r], dev(dy=r)
        ).wait_recv()
    wc = wc_v[...].reshape(NY * HD, GW)

    outs = []
    for n, quarter in enumerate(order):
        d = quarter // 2
        y_copy(1 - d, n, quarter, False).wait_recv()
        y_copy(d, 4 + quarter % 2, quarter, False).wait_recv()
        att = jnp.concatenate([att_v[h, rows_of(quarter), :] for h in range(NY)], axis=1)
        cross = jnp.dot(att, wc, preferred_element_type=F32)
        mixed = pool_v[rows_of(quarter), :] + gate_v[rows_of(quarter), :] * cross
        out_v[rows_of(quarter), :] = mixed.astype(BF)
        outs.append(local(out_v.at[rows_of(quarter)], out_h.at[rows_of(quarter)], osem.at[n]))

    for cp in sends:
        cp.wait_send()
    for cp in outs:
        cp.wait()


def per_device(
    tokens, passage_ids, store, mix_gain, w_query, w_key, w_value, w_cross_out,
    head_scale, w_pool_in, w_pool_mix, pool_scale, gate_weight,
):
    anywhere = pl.BlockSpec(memory_space=pl.ANY)
    dma = pltpu.SemaphoreType.DMA
    in_specs = [anywhere] * 13
    in_specs[8] = pl.BlockSpec(memory_space=pltpu.SMEM)
    v = pltpu.VMEM
    return pl.pallas_call(
        kernel,
        out_shape=jax.ShapeDtypeStruct((ROWS, GW), BF),
        in_specs=in_specs,
        out_specs=anywhere,
        scratch_shapes=[
            v((ROWS, D), BF),
            v((OWN, PLEN, D), BF),
            v((D, 2 * HD), BF),
            v((D, HD), BF),
            v((D, GW), BF),
            v((GW, GW), BF),
            v((1, D), BF),
            v((NY, GW), BF),
            v((NY, GW), F32),
            v((SLOTS, HD, PLEN), BF),
            v((SLOTS, PLEN, HD), BF),
            v((NX, ROWS, HD), BF),
            v((NX, NBLK, NPB), jnp.int32),
            pltpu.SMEM((NX, NBLK, NPB), jnp.int32),
            v((NY, HD, GW), BF),
            v((ROWS, GW), BF),
            v((ROWS, GW), F32),
            v((ROWS, GW), F32),
            v((NX, ROWS, NPB * PLEN), BF),
            v((NX, ROWS, HD), BF),
            v((2, ROWS // 2, HD), BF),
            v((2, ROWS // 2, HD), BF),
            v((2, ROWS, HD), BF),
            v((NX, 8, 128), F32),
            v((NX, 8, 128), F32),
            v((NY, ROWS, HD), BF),
            v((ROWS, GW), BF),
            dma((12,)),
            dma((ROWS // TCHUNK,)),
            dma((4,)),
            dma((16,)), dma((16,)),
            dma((16,)), dma((16,)),
            dma((6,)), dma((6,)),
            dma((4,)), dma((4,)),
            dma((4,)), dma((4,)),
            dma((4,)), dma((4,)),
            dma((12,)), dma((12,)),
            dma((12,)), dma((12,)),
        ],
        compiler_params=pltpu.CompilerParams(
            collective_id=0, has_side_effects=True, vmem_limit_bytes=60 * 1024 * 1024
        ),
        name="mixer",
    )(
        tokens, passage_ids, store, mix_gain.reshape(1, D), w_query, w_key, w_value, w_cross_out,
        head_scale, w_pool_in, w_pool_mix, pool_scale.reshape(NY, GW), gate_weight.reshape(NY, GW),
    )


def solution(mesh):
    return jax.shard_map(
        per_device,
        mesh=mesh,
        in_specs=(
            P("st", None),
            P("st", None),
            P("st", None, None),
            P(),
            P(None, "tp"),
            P(None, "tp"),
            P(None, "tp"),
            P("tp", None),
            P(),
            P(None, "tp"),
            P(),
            P(),
            P(),
        ),
        out_specs=P("st", "tp"),
        check_vma=False,
    )
```

time: 230 us -> 70.1 us (0.30)
  waiting for transfers between devices: 102 us -> 0 us
  Pallas kernels: 0 us -> 62.8 us
  starting transfers between devices: 40.2 us -> 0 us
  matrix products: 33.9 us -> 0 us
  local copies, waits for them, and re-layouts: 31 us -> 7.07 us
  other arithmetic: 19.6 us -> 0 us
    all_to_all x5 -> x0, waiting for transfers between devices: 102 us -> none  [the longest x1 50.4 us: per_device(): lax.all_to_all(partial_out, 'st', split_axis=0, concat_axis=0, tiled=True)]
    pallas_call x0 -> x1, Pallas kernels: none -> 62.8 us  [per_device(): pl.pallas_call(kernel, out_shape=jax.ShapeDtypeStruct((ROWS, GW), BF), in...]
    all_to_all x5 -> x0, starting transfers between devices: 40.2 us -> none  [the longest x1 11.9 us: per_device(): lax.all_to_all(requests, 'st', split_axis=0, concat_axis=0, tiled=True)]
    dot_general x8 -> x0, matrix products: 33.9 us -> none  [the longest x1 8.43 us: per_device(): jnp.einsum('scqhd,sckhd->schqk', got_queries, chosen_keys, preferred_elem...]
    gather x5 -> x0, local copies, waits for them, and re-layouts: 11.6 us -> none  [the longest x1 3.25 us: per_device(): back_out.reshape(st_size * capacity, block_rows, heads_local, HEAD_DIM)]
    reduce_sum x5 -> x0, other arithmetic: 9.94 us -> none  [the longest x1 5.22 us: per_device(): jnp.mean(floats * floats, axis=-1, keepdims=True) + EPSILON]
    scatter x2 -> x0, local copies, waits for them, and re-layouts: 9.87 us -> none  [the longest x1 9.1 us: per_device(): query_buffer = jnp.zeros((st_size * capacity, block_rows, heads_local * H...]
    convert_element_type x9 -> x0, other arithmetic: 5.22 us -> none  [the longest x1 3.14 us: pool_residual(): return result.reshape(row_count, chan_width).astype(jnp.bfloat16)]
  transfers between devices with their start and end apart: 5 -> 0, of which waited for: 4 -> 0; matrix products, arithmetic and copies ran while one was open for 24% -> 0% of each run, Pallas kernels for 0% -> 0%
where the time goes in v1:
time: 70.1 us; the launch traced here: 69.8 us
  Pallas kernels  62.8 us (90%)
  local copies, waits for them, and re-layouts  7.07 us (10%)
    pallas_call x1, Pallas kernels, per_device(): pl.pallas_call(kernel, out_shape=jax.ShapeDtypeStruct((ROWS, GW), BF), in...  62.8 us
    unnamed x2, local copies, waits for them, and re-layouts  3.22 us

profile of v1, /device:TPU:8, one launch (start us, length us, event | category | flops | bytes accessed | tf_op | source)
XLA Modules:
  0.0 69.8 jit_solution(14699427546410292533)
XLA Ops:
  0.0 1.3 %reshape.10.ps_h = bf16[4,256]{1,0:T(4,128)(2,1)} reshape(bf16[1024]{0:T(1024)(128)(2,1)} %param.24) | data formatting | bytes 4096 | tf_op jit(solution)/shard_map/reshape | solution.py:510
  1.3 1.3 %reshape.11.gw_h = f32[4,256]{1,0:T(4,128)} reshape(f32[1024]{0:T(1024)} %param.25) | data formatting | bytes 8192 | tf_op jit(solution)/shard_map/reshape | solution.py:510
  2.5 1.3 %copy.14.ids_h = s32[16,4]{1,0:T(8,128)} copy(s32[16,4]{0,1:T(4,128)} %param.14) | data formatting | bytes 512 | tf_op args[1]
  3.9 1.3 %reshape.9.gain_h = bf16[1,4096]{1,0:T(2,128)(2,1)} reshape(bf16[4096]{0:T(1024)(128)(2,1)} %param.16) | data formatting | bytes 16384 | tf_op jit(solution)/shard_map/reshape | solution.py:509
  5.2 62.8 %mixer.1 = bf16[1024,256]{1,0:T(8,128)(2,1)} custom-call(bf16[1024,4096]{1,0:T(8,128)(2,1)} %tok_h.1, s32[16,4]{1,0:T(8,128)} %copy.14.ids_h, bf16[3,128,4096]{2,1,0:T(8,128)(2,1)} %store_h.1, bf16[1,4096]{1,0:T(2,128)(2,1)} %reshape.9.gain_h, bf16[4096,128]{1,0:T(8,128)(2,1)} %wq_h.1, bf16[4096,128]{1,0:T(8,128)(2,1)} %wk_h.1, bf16[4096,128]{1,0:T(8,128)(2,1)} %wv_h.1, ...), custom_call_target="tpu_custom_call" | custom-call | tf_op jit(solution)/shard_map/mixer/pallas_call | solution.py:459
  68.0 1.9 %copy.16 = bf16[1024,256]{1,0:T(8,128)(2,1)} copy(bf16[1024,256]{1,0:T(8,128)(2,1)} %mixer.1) | data formatting | bytes 1048576

commit v2 on v1

v2 whole, which is shorter than its diff:
```python
import functools
import math

import jax
import jax.numpy as jnp
from jax import lax
from jax.experimental import pallas as pl
from jax.experimental.pallas import tpu as pltpu
from jax.sharding import PartitionSpec as P

MESH = pl.DeviceIdType.MESH
BF = jnp.bfloat16
F32 = jnp.float32

EPSILON = 1e-06
NZ, NX, NC, NY = 8, 4, 2, 4
D = 4096
HD = 128
GW = 256
ROWS = 1024
BLOCK = 64
NPB = 4
NBLK = 16
PLEN = 128
OWN = 3
SEQ = 128
SLOTS = NZ * NC * OWN
TCHUNK = 256
STEP = 128

Z_ORDER = tuple(
    tuple((n // 100, n // 10 % 10, n % 10) for n in codes)
    for codes in (
        (1, 0, 101, 2, 100, 10, 11, 12, 102, 20, 21, 110, 22, 30, 31, 111, 112, 120, 121, 122, 130),
        (1, 0, 2, 102, 101, 10, 12, 11, 100, 111, 22, 21, 20, 112, 32, 121, 110, 122, 131, 120, 132),
    )
)


def kernel(
    tok_h, ids_h, store_h, gain_h, wq_h, wk_h, wv_h, wc_h, hs_s, wp_h, wm_h, ps_h, gw_h,
    out_h,
    tok_v, store_v, wkv_v, wqp_v, wm_v, gain_v, ps_v, gw_v,
    kt_v, v_v, qg_v, idv, tbl_v, tbl_s, wc_v,
    pooled_v, pool_v, gate_v, e_v, part_v, rly_v, sum_v, rrecv_v, tot_v, totg_v, att_v, out_v,
    lsem, tsem, osem,
    zs, zr, cs, cr, qs, qr, ids_ss, ids_rs, wcs, wcr, ts, tr, rs, rr, ys, yr,
):
    s = lax.axis_index("st")
    y = lax.axis_index("tp")
    c = lax.rem(s, NC)
    x = lax.rem(lax.div(s, NC), NX)
    z = lax.div(s, NC * NX)

    def dev(dz=0, dx=0, dy=0, other=False):
        cc = 1 - c if other else c
        zz = lax.rem(z + dz + NZ, NZ)
        xx = lax.rem(x + dx + NX, NX)
        yy = lax.rem(y + dy + NY, NY)
        return (zz * (NX * NC) + xx * NC + cc, yy)

    def remote(src, dst, ssem, rsem, to):
        return pltpu.make_async_remote_copy(
            src_ref=src, dst_ref=dst, send_sem=ssem, recv_sem=rsem,
            device_id=to, device_id_type=MESH,
        )

    barrier = pltpu.get_barrier_semaphore()
    partners = [
        dev(dz=1), dev(dz=-1), dev(dx=1), dev(dx=-1), dev(dx=2),
        dev(dy=1), dev(dy=-1), dev(dy=2), dev(other=True),
    ]
    for to in partners:
        pl.semaphore_signal(barrier, inc=1, device_id=to, device_id_type=MESH)

    def local(src, dst, sem):
        copy = pltpu.make_async_copy(src, dst, sem)
        copy.start()
        return copy

    kv_loads = []
    for h in (0, 1):
        part = pl.ds(h * (D // 2), D // 2)
        kv_loads.append([
            local(wk_h.at[part], wkv_v.at[part, pl.ds(0, HD)], lsem.at[3 * h]),
            local(wv_h.at[part], wkv_v.at[part, pl.ds(HD, HD)], lsem.at[3 * h + 1]),
            local(store_h.at[:, :, part], store_v.at[:, :, part], lsem.at[3 * h + 2]),
        ])

    def kv_half(h):
        half = slice(h * (D // 2), (h + 1) * (D // 2))
        return jnp.dot(
            store_v[:, :, half].reshape(OWN * PLEN, D // 2), wkv_v[half, :],
            preferred_element_type=F32,
        )

    for load in kv_loads[0]:
        load.wait()
    kv = kv_half(0)
    for load in kv_loads[1]:
        load.wait()
    gain_load = local(gain_h, gain_v, lsem.at[6])
    wq_load = local(wq_h, wqp_v.at[:, pl.ds(0, HD)], lsem.at[7])
    wp_load = local(wp_h, wqp_v.at[:, pl.ds(HD, GW)], lsem.at[8])
    tok_loads = []
    for i in range(ROWS // TCHUNK):
        chunk = pl.ds(i * TCHUNK, TCHUNK)
        tok_loads.append(local(tok_h.at[chunk], tok_v.at[chunk], tsem.at[i]))
    pool_loads = [
        local(wm_h.at[y], wm_v, lsem.at[9]),
        local(ps_h, ps_v, lsem.at[10]),
        local(gw_h, gw_v, lsem.at[11]),
    ]
    ids_own = local(ids_h, idv.at[0], lsem.at[12])
    wc_own = local(
        wc_h.at[:, pl.ds(pl.multiple_of(y * GW, GW), GW)], wc_v.at[y], lsem.at[13]
    )
    kv = kv + kv_half(1)
    keys = kv[:, :HD]
    keys = keys * lax.rsqrt(jnp.mean(keys * keys, axis=-1, keepdims=True) + EPSILON)
    own_slot = (z * NC + c) * OWN
    for i in range(OWN):
        rows = slice(i * PLEN, (i + 1) * PLEN)
        kt_v[own_slot + i] = jnp.transpose(keys[rows]).astype(BF)
        v_v[own_slot + i] = kv[rows, HD:].astype(BF)

    pl.semaphore_wait(barrier, len(partners))
    sends = []
    bufs = (kt_v, v_v)

    last = (((0, 0), (0, 1), (1, 0)), ((0, 2), (1, 1), (1, 2)))

    def z_copy(d, item, sending):
        kind, k, i = item
        sign = 1 if d == 0 else -1
        origin = lax.rem(z - sign * (k if sending else k + 1) + NZ, NZ)
        block = bufs[kind].at[(origin * NC + c) * OWN + i]
        n = ((d * 2 + kind) * 4 + k) * OWN + i
        return remote(block, block, zs.at[n], zr.at[n], dev(dz=sign))

    def core_copy(kind, o, core):
        block = bufs[kind].at[pl.ds((lax.rem(z + o, NZ) * NC + core) * OWN, OWN)]
        n = kind * NZ + o
        return remote(block, block, cs.at[n], cr.at[n], dev(other=True))

    def core_send(kind, o):
        cp = core_copy(kind, o, c)
        cp.start()
        sends.append(cp)

    arrived = set()

    def z_wait(d, item):
        if (d, item) in arrived:
            return
        arrived.add((d, item))
        z_copy(d, item, False).wait_recv()
        kind, k, _ = item
        if k < 3:
            if all((d, (kind, k, i)) in arrived for i in range(OWN)):
                core_send(kind, k + 1 if d == 1 else NZ - k - 1)
        elif all(
            (dd, (kind, 3, i)) in arrived for dd in (0, 1) for kk, i in last[dd] if kk == kind
        ):
            core_send(kind, 4)

    def z_step(n):
        for d in (0, 1):
            item = Z_ORDER[d][n]
            kind, k, i = item
            if k:
                z_wait(d, (kind, k - 1, i))
            cp = z_copy(d, item, True)
            cp.start()
            sends.append(cp)

    def z_finish(kind):
        for k in (2, 3):
            for d in (0, 1):
                for i in range(OWN):
                    if k == 2 or (kind, i) in last[d]:
                        z_wait(d, (kind, k, i))
        for o in range(NZ):
            core_copy(kind, o, 1 - c).wait_recv()

    for n in range(5):
        z_step(n)
    for kind in (0, 1):
        core_send(kind, 0)

    for r in (1, 2, 3):
        cp = remote(ids_h, idv.at[NX - r], ids_ss.at[r], ids_rs.at[NX - r], dev(dx=r))
        cp.start()
        sends.append(cp)
    for r in (1, 2, 3):
        column = pl.multiple_of(lax.rem(y + r, NY) * GW, GW)
        cp = remote(
            wc_h.at[:, pl.ds(column, GW)], wc_v.at[y], wcs.at[r], wcr.at[NY - r], dev(dy=r)
        )
        cp.start()
        sends.append(cp)

    gain_load.wait()
    wq_load.wait()
    wp_load.wait()
    gain = gain_v[...].reshape(1, D)

    def q_copy(d, m, sending):
        sign = 1 if d == 0 else -1
        if m < 2:
            half, back = m, 0
        else:
            half, back = d, 1
        origin = back if sending else back + 1
        row = (origin if d == 1 else NX - origin) % NX
        at = qg_v.at[row, pl.ds(half * (ROWS // 2), ROWS // 2)]
        back_there = back + 1
        row_there = (back_there if d == 1 else NX - back_there) % NX
        to = qg_v.at[row_there, pl.ds(half * (ROWS // 2), ROWS // 2)] if sending else at
        i = d * 3 + m
        return remote(at, to, qs.at[i], qr.at[i], dev(dx=sign))

    def q_send(d, m):
        cp = q_copy(d, m, True)
        cp.start()
        sends.append(cp)

    def token_chunk(i):
        tok_loads[i].wait()
        chunk = pl.ds(i * TCHUNK, TCHUNK)
        t = tok_v[chunk, :]
        tf = t.astype(F32)
        scale = lax.rsqrt(jnp.mean(tf * tf, axis=-1, keepdims=True) + EPSILON)
        both = jnp.dot(t * gain, wqp_v[...], preferred_element_type=F32) * scale
        q = both[:, :HD]
        q = q * lax.rsqrt(jnp.mean(q * q, axis=-1, keepdims=True) + EPSILON)
        qg_v[0, chunk, :] = q.astype(BF)
        pooled_v[chunk, :] = both[:, HD:].astype(BF)

    token_chunk(0)
    token_chunk(1)
    for d in (0, 1):
        q_send(d, 0)
    for n in (5, 6, 7, 8):
        z_step(n)
    token_chunk(2)
    for n in (9, 10):
        z_step(n)
    token_chunk(3)
    for d in (0, 1):
        q_send(d, 1)
    ids_own.wait()
    for r in (1, 2, 3):
        remote(ids_h, idv.at[r], ids_ss.at[r], ids_rs.at[r], dev(dx=r)).wait_recv()
    p = idv[...]
    owner = lax.shift_right_logical(p * 171, 9)
    place = lax.shift_right_logical(owner, 3) * NC + (owner & 1)
    tbl_v[0] = place * OWN + (p - owner * OWN)
    tbl_v[1] = jnp.where((lax.shift_right_logical(owner, 1) & 3) == x, 1, 0)
    tbl_load = local(tbl_v, tbl_s, lsem.at[14])
    for n in (11, 12, 13, 14):
        z_step(n)
    q_copy(0, 0, False).wait_recv()
    q_send(0, 2)
    tbl_load.wait()
    for n in (15, 16, 17):
        z_step(n)
    z_finish(0)
    q_copy(1, 1, False).wait_recv()
    q_send(1, 2)
    scale = hs_s[y] * (math.log2(math.e) / math.sqrt(HD))
    row_id = lax.broadcasted_iota(jnp.int32, (SEQ, SEQ), 0)
    col_id = lax.broadcasted_iota(jnp.int32, (SEQ, SEQ), 1)
    eye = row_id == col_id

    def slot_of(r, b, j):
        return tbl_s[0, r, j, b], tbl_s[1, r, j, b] == 1

    def score_pair(r, pair):
        totals = []
        for u in (0, 1):
            b = pair * 2 + u
            q = qg_v[r, pl.ds(pl.multiple_of(b * BLOCK, BLOCK), BLOCK), :]
            found = [slot_of(r, b, j) for j in range(NPB)]
            kt = jnp.concatenate([kt_v[slot] for slot, _ in found], axis=1)
            sc = jnp.dot(q, kt, preferred_element_type=F32)
            e = jnp.exp2(sc * scale)
            es = [
                jnp.where(found[j][1], e[:, j * PLEN : (j + 1) * PLEN], 0.0) for j in range(NPB)
            ]
            at = pl.multiple_of(b * BLOCK, BLOCK)
            for j in range(NPB):
                e_v[r, pl.ds(at, BLOCK), pl.ds(j * PLEN, PLEN)] = es[j].astype(BF)
            both = (es[0] + es[1]) + (es[2] + es[3])
            totals.append(jnp.sum(both, axis=1, keepdims=True))
        column = jnp.concatenate(totals, axis=0)
        row = jnp.sum(jnp.where(eye, column, 0.0), axis=0, keepdims=True)
        tot_v[r, pl.ds(pair, 1), :] = row

    def score_all(r):
        def score_body(i, carry):
            for u in range(4):
                score_pair(r, i * 4 + u)
            return carry

        lax.fori_loop(0, NBLK // 8, score_body, 0)
        if r:
            cp = remote(tot_v.at[r], totg_v.at[NX - r], ts.at[r], tr.at[NX - r], dev(dx=r))
            cp.start()
            sends.append(cp)

    score_all(0)
    z_step(18)
    q_copy(1, 0, False).wait_recv()
    score_all(1)
    z_step(19)
    q_copy(0, 1, False).wait_recv()
    score_all(3)
    z_step(20)
    for d in (0, 1):
        q_copy(d, 2, False).wait_recv()
    score_all(2)
    z_finish(1)

    def step_rows(d, i):
        return pl.ds(d * (ROWS // 2) + i * STEP, STEP)

    def values(pairs):
        for r, d, i in pairs:
            for u in range(STEP // BLOCK):
                b = d * (NBLK // 2) + i * (STEP // BLOCK) + u
                rows = pl.ds(b * BLOCK, BLOCK)
                vv = jnp.concatenate([v_v[slot_of(r, b, j)[0]] for j in range(NPB)], axis=0)
                o = jnp.dot(e_v[r, rows, :], vv, preferred_element_type=F32)
                part_v[r, rows, :] = o.astype(BF)

    def r_copy(d, m, i, src, dst):
        n = (d * 3 + m) * 4 + i
        return remote(src, dst, rs.at[n], rr.at[n], dev(dx=1 if d == 0 else -1))

    def r_send(d, m, i, src, dst):
        cp = r_copy(d, m, i, src, dst)
        cp.start()
        sends.append(cp)

    near = (1, 3)

    def far(i):
        values([(2, 0, i), (2, 1, i)])
        for d in (0, 1):
            here = pl.ds(i * STEP, STEP)
            r_send(d, 0, i, part_v.at[2, step_rows(d, i)], rly_v.at[d, here])

    def direct(i):
        values([(near[0], 1, i), (near[1], 0, i)])
        for d in (0, 1):
            rows = step_rows(1 - d, i)
            r_send(d, 1, i, part_v.at[near[d], rows], rrecv_v.at[d, rows])

    def relayed(i):
        values([(near[0], 0, i), (near[1], 1, i)])

    def own(i):
        values([(0, 0, i), (0, 1, i)])

    def relay(i):
        for d in (0, 1):
            rows = step_rows(d, i)
            here = pl.ds(i * STEP, STEP)
            r_copy(d, 0, i, part_v.at[2, rows], rly_v.at[d, here]).wait_recv()
            both = rly_v[d, here, :].astype(F32) + part_v[near[d], rows, :].astype(F32)
            sum_v[d, here, :] = both.astype(BF)
            r_send(d, 2, i, sum_v.at[d, here], rrecv_v.at[d, rows])

    def y_copy(d, m, half, i, sending):
        sign = 1 if d == 0 else -1
        back = (0 if m < 2 else 1) + (0 if sending else 1)
        head = lax.rem(y - sign * back + NY, NY)
        block = att_v.at[head, step_rows(half, i)]
        n = (d * 3 + m) * 4 + i
        return remote(block, block, ys.at[n], yr.at[n], dev(dy=sign))

    def y_send(d, m, half, i):
        cp = y_copy(d, m, half, i, True)
        cp.start()
        sends.append(cp)

    def attend(i):
        for half in (0, 1):
            rows = step_rows(half, i)
            for d in (0, 1):
                m = 2 if d == half else 1
                r_copy(d, m, i, rrecv_v.at[d, rows], rrecv_v.at[d, rows]).wait_recv()
            pair = half * 4 + i
            row = tot_v[0, pair : pair + 1, :]
            for r in (1, 2, 3):
                row = row + totg_v[r, pair : pair + 1, :]
            total = jnp.sum(jnp.where(eye, row, 0.0), axis=1, keepdims=True)
            summed = (
                part_v[0, rows, :].astype(F32)
                + rrecv_v[0, rows, :].astype(F32)
                + rrecv_v[1, rows, :].astype(F32)
            )
            att_v[y, rows, :] = (summed * (1.0 / total)).astype(BF)
            for d in (0, 1):
                y_send(d, half, half, i)

    def y_forward(i):
        for d in (0, 1):
            y_copy(d, d, d, i, False).wait_recv()
            y_send(d, 2, d, i)

    far(0)
    far(1)
    direct(0)
    relayed(0)
    far(2)
    relay(0)
    direct(1)
    relayed(1)
    far(3)
    relay(1)
    direct(2)
    relayed(2)
    own(0)
    relay(2)
    direct(3)
    relayed(3)
    own(1)
    for r in (1, 2, 3):
        remote(tot_v.at[r], totg_v.at[r], ts.at[r], tr.at[r], dev(dx=r)).wait_recv()
    attend(0)
    relay(3)
    own(2)
    own(3)
    for load in pool_loads:
        load.wait()
    window = lax.shift_left(jnp.int32(2), y.astype(jnp.int32))
    band = jnp.where((col_id <= row_id) & (col_id > row_id - window), 1.0, 0.0).astype(BF)
    position = lax.broadcasted_iota(jnp.int32, (SEQ, GW), 0)
    inverse = 1.0 / jnp.minimum(position + 1, window).astype(F32)
    ps_all = ps_v[...].astype(F32).reshape(1, NY * GW)
    gw_all = gw_v[...].reshape(1, NY * GW)
    ps = jnp.zeros((1, GW), F32)
    gw = jnp.zeros((1, GW), F32)
    for g in range(NY):
        here = y == g
        ps = ps + jnp.where(here, ps_all[:, g * GW : (g + 1) * GW], 0.0)
        gw = gw + jnp.where(here, gw_all[:, g * GW : (g + 1) * GW], 0.0)

    def pool_step(i):
        rows = pl.ds(i * SEQ, SEQ)
        p = pooled_v[rows, :]
        pf = p.astype(F32)
        sums = jnp.dot(band, p, preferred_element_type=F32)
        residual = (sums * inverse - pf).astype(BF)
        pool_v[rows, :] = jnp.dot(residual, wm_v[...], preferred_element_type=F32) * ps
        gate_v[rows, :] = 1.0 / (1.0 + jnp.exp(-(pf * gw)))

    pool_step(0)
    pool_step(4)
    attend(1)
    pool_step(1)
    pool_step(5)
    attend(2)
    y_forward(0)
    attend(3)
    y_forward(1)
    pool_step(2)
    pool_step(6)
    y_forward(2)
    pool_step(3)
    pool_step(7)
    wc_own.wait()
    for r in (1, 2, 3):
        remote(
            wc_h.at[:, pl.ds(0, GW)], wc_v.at[lax.rem(y + r, NY)], wcs.at[r], wcr.at[r], dev(dy=r)
        ).wait_recv()
    wc = wc_v[...].reshape(NY * HD, GW)

    outs = []

    def cross(i):
        for half in (0, 1):
            rows = step_rows(half, i)
            y_copy(1 - half, half, half, i, False).wait_recv()
            y_copy(half, 2, half, i, False).wait_recv()
            att = jnp.concatenate([att_v[h, rows, :] for h in range(NY)], axis=1)
            term = jnp.dot(att, wc, preferred_element_type=F32)
            mixed = pool_v[rows, :] + gate_v[rows, :] * term
            out_v[rows, :] = mixed.astype(BF)
            outs.append(local(out_v.at[rows], out_h.at[rows], osem.at[half * 4 + i]))

    cross(0)
    y_forward(3)
    cross(1)
    cross(2)
    cross(3)
    for cp in sends:
        cp.wait_send()
    for cp in outs:
        cp.wait()


def per_device(
    tokens, passage_ids, store, mix_gain, w_query, w_key, w_value, w_cross_out,
    head_scale, w_pool_in, w_pool_mix, pool_scale, gate_weight,
):
    anywhere = pl.BlockSpec(memory_space=pl.ANY)
    dma = pltpu.SemaphoreType.DMA
    in_specs = [anywhere] * 13
    in_specs[8] = pl.BlockSpec(memory_space=pltpu.SMEM)
    v = pltpu.VMEM
    return pl.pallas_call(
        kernel,
        out_shape=jax.ShapeDtypeStruct((ROWS, GW), BF),
        in_specs=in_specs,
        out_specs=anywhere,
        scratch_shapes=[
            v((ROWS, D), BF),
            v((OWN, PLEN, D), BF),
            v((D, 2 * HD), BF),
            v((D, HD + GW), BF),
            v((GW, GW), BF),
            v((D,), BF),
            v((NY * GW,), BF),
            v((NY * GW,), F32),
            v((SLOTS, HD, PLEN), BF),
            v((SLOTS, PLEN, HD), BF),
            v((NX, ROWS, HD), BF),
            v((NX, NPB, NBLK), jnp.int32),
            v((2, NX, NPB, NBLK), jnp.int32),
            pltpu.SMEM((2, NX, NPB, NBLK), jnp.int32),
            v((NY, HD, GW), BF),
            v((ROWS, GW), BF),
            v((ROWS, GW), F32),
            v((ROWS, GW), F32),
            v((NX, ROWS, NPB * PLEN), BF),
            v((NX, ROWS, HD), BF),
            v((2, ROWS // 2, HD), BF),
            v((2, ROWS // 2, HD), BF),
            v((2, ROWS, HD), BF),
            v((NX, 8, 128), F32),
            v((NX, 8, 128), F32),
            v((NY, ROWS, HD), BF),
            v((ROWS, GW), BF),
            dma((15,)),
            dma((ROWS // TCHUNK,)),
            dma((8,)),
            dma((48,)), dma((48,)),
            dma((16,)), dma((16,)),
            dma((6,)), dma((6,)),
            dma((4,)), dma((4,)),
            dma((4,)), dma((4,)),
            dma((4,)), dma((4,)),
            dma((24,)), dma((24,)),
            dma((24,)), dma((24,)),
        ],
        compiler_params=pltpu.CompilerParams(
            collective_id=0, has_side_effects=True, vmem_limit_bytes=60 * 1024 * 1024
        ),
        name="mixer",
    )(
        tokens, passage_ids.T, store, mix_gain, w_query, w_key, w_value, w_cross_out,
        head_scale, w_pool_in, w_pool_mix, pool_scale, gate_weight,
    )


def solution(mesh):
    return jax.shard_map(
        per_device,
        mesh=mesh,
        in_specs=(
            P("st", None),
            P("st", None),
            P("st", None, None),
            P(),
            P(None, "tp"),
            P(None, "tp"),
            P(None, "tp"),
            P("tp", None),
            P(),
            P(None, "tp"),
            P(),
            P(),
            P(),
        ),
        out_specs=P("st", "tp"),
        check_vma=False,
    )
```

time: 70.1 us -> 61.6 us (0.88)
  local copies, waits for them, and re-layouts: 7.07 us -> 1.87 us
  Pallas kernels: 62.8 us -> 59.6 us
    reshape x3 -> x0, local copies, waits for them, and re-layouts: 3.85 us -> none  [the longest x1 1.31 us: per_device(): mix_gain.reshape(1, D)]
    pallas_call x1, Pallas kernels: 62.8 us -> 59.6 us  [per_device(): pl.pallas_call(kernel, out_shape=jax.ShapeDtypeStruct((ROWS, GW), BF), in...]
    unnamed x2 -> x1, local copies, waits for them, and re-layouts: 3.22 us -> 1.87 us
where the time goes in v2:
time: 61.6 us; the launch traced here: 61.5 us
  Pallas kernels  59.6 us (97%)
  local copies, waits for them, and re-layouts  1.87 us (3%)
    pallas_call x1, Pallas kernels, per_device(): pl.pallas_call(kernel, out_shape=jax.ShapeDtypeStruct((ROWS, GW), BF), in...  59.6 us
    unnamed x1, local copies, waits for them, and re-layouts  1.87 us

profile of v2, /device:TPU:8, one launch (start us, length us, event | category | flops | bytes accessed | tf_op | source)
XLA Modules:
  0.0 61.5 jit_solution(3929986696348617080)
XLA Ops:
  0.0 59.6 %mixer.1 = bf16[1024,256]{1,0:T(8,128)(2,1)} custom-call(bf16[1024,4096]{1,0:T(8,128)(2,1)} %tok_h.1, s32[4,16]{1,0:T(4,128)} %bitcast.1, bf16[3,128,4096]{2,1,0:T(8,128)(2,1)} %store_h.1, bf16[4096]{0:T(1024)(128)(2,1)} %gain_h.1, bf16[4096,128]{1,0:T(8,128)(2,1)} %wq_h.1, bf16[4096,128]{1,0:T(8,128)(2,1)} %wk_h.1, bf16[4096,128]{1,0:T(8,128)(2,1)} %wv_h.1, ...), custom_call_target="tpu_custom_call" | custom-call | tf_op jit(solution)/shard_map/mixer/pallas_call | solution.py:514
  59.6 1.9 %copy.15 = bf16[1024,256]{1,0:T(8,128)(2,1)} copy(bf16[1024,256]{1,0:T(8,128)(2,1)} %mixer.1) | data formatting | bytes 1048576

commit v3 on v2

v3 whole, which is shorter than its diff:
```python
import functools
import math

import jax
import jax.numpy as jnp
from jax import lax
from jax.experimental import pallas as pl
from jax.experimental.pallas import tpu as pltpu
from jax.sharding import PartitionSpec as P

MESH = pl.DeviceIdType.MESH
BF = jnp.bfloat16
F32 = jnp.float32

EPSILON = 1e-06
NZ, NX, NC, NY = 8, 4, 2, 4
D = 4096
HD = 128
GW = 256
ROWS = 1024
BLOCK = 64
NPB = 4
NBLK = 16
PLEN = 128
OWN = 3
SEQ = 128
SLOTS = NZ * NC * OWN
TCHUNK = 256
PIECES = ROWS // TCHUNK * 2
KVP = 4
STEP = 128

SENT_ROWS = (
    42 * PLEN * HD + 16 * OWN * PLEN * HD + 6 * (ROWS // 2) * HD + 3 * HD * GW
    + 2 * 24 * STEP * HD
) // D

Z_ORDER = tuple(
    tuple((n // 100, n // 10 % 10, n % 10) for n in codes)
    for codes in (
        (1, 0, 101, 2, 100, 10, 11, 12, 102, 20, 21, 110, 22, 30, 31, 111, 112, 120, 121, 122, 130),
        (1, 0, 2, 102, 101, 10, 12, 11, 100, 111, 22, 21, 20, 112, 32, 121, 110, 122, 131, 120, 132),
    )
)


def kernel(
    tok_h, ids_h, store_h, gain_h, wq_h, wk_h, wv_h, wc_h, hs_s, wp_h, wm_h, ps_h, gw_h,
    out_h,
    tok_v, store_v, wkv_v, wqp_v, kv_v, acc_v, sq_v, wm_v, gain_v, ps_v, gw_v,
    kt_v, v_v, qg_v, idv, tbl_v, tbl_s, wc_v,
    pooled_v, pool_v, gate_v, e_v, part_v, rly_v, sum_v, rrecv_v, tot_v, totg_v, att_v, out_v,
    lsem, tsem, osem,
    ss, zr, cr, qr, ids_ss, ids_rs, wcr, ts, tr, rr, yr,
):
    s = lax.axis_index("st")
    y = lax.axis_index("tp")
    c = lax.rem(s, NC)
    x = lax.rem(lax.div(s, NC), NX)
    z = lax.div(s, NC * NX)

    def dev(dz=0, dx=0, dy=0, other=False):
        cc = 1 - c if other else c
        zz = lax.rem(z + dz + NZ, NZ)
        xx = lax.rem(x + dx + NX, NX)
        yy = lax.rem(y + dy + NY, NY)
        return (zz * (NX * NC) + xx * NC + cc, yy)

    def remote(src, dst, ssem, rsem, to):
        return pltpu.make_async_remote_copy(
            src_ref=src, dst_ref=dst, send_sem=ssem, recv_sem=rsem,
            device_id=to, device_id_type=MESH,
        )

    barrier = pltpu.get_barrier_semaphore()
    partners = [
        dev(dz=1, other=True), dev(dz=-1, other=True), dev(dx=1), dev(dx=-1), dev(dx=2),
        dev(dy=1), dev(dy=-1), dev(dy=2), dev(other=True),
    ]
    for to in partners:
        pl.semaphore_signal(barrier, inc=1, device_id=to, device_id_type=MESH)

    def local(src, dst, sem):
        copy = pltpu.make_async_copy(src, dst, sem)
        copy.start()
        return copy

    for h in range(KVP):
        part = pl.ds(h * (D // KVP), D // KVP)
        local(wk_h.at[part], wkv_v.at[part, pl.ds(0, HD)], lsem.at[2 * h])
        local(wv_h.at[part], wkv_v.at[part, pl.ds(HD, HD)], lsem.at[2 * h])
        local(store_h.at[:, :, part], store_v.at[:, :, part], lsem.at[2 * h + 1])

    def landed(ref, sem):
        pltpu.make_async_copy(ref, ref, sem).wait()

    def kv_part(h):
        part = pl.ds(h * (D // KVP), D // KVP)
        landed(wkv_v.at[part], lsem.at[2 * h])
        landed(store_v.at[:, :, part], lsem.at[2 * h + 1])
        term = jnp.dot(
            store_v[:, :, part].reshape(OWN * PLEN, D // KVP), wkv_v[part, :],
            preferred_element_type=F32,
        )
        kv_v[...] = term if h == 0 else kv_v[...] + term

    kv_part(0)
    kv_part(1)
    kv_part(2)
    kv_part(3)
    gain_load = local(gain_h, gain_v, lsem.at[8])
    local(wq_h, wqp_v.at[:, pl.ds(0, HD)], lsem.at[9])
    local(wp_h, wqp_v.at[:, pl.ds(HD, GW)], lsem.at[9])
    tok_loads = []
    for i in range(PIECES):
        part = (pl.ds(i // 2 * TCHUNK, TCHUNK), pl.ds(i % 2 * (D // 2), D // 2))
        tok_loads.append(local(tok_h.at[part], tok_v.at[part], tsem.at[i]))
    pool_loads = [
        local(wm_h.at[y], wm_v, lsem.at[10]),
        local(ps_h, ps_v, lsem.at[11]),
        local(gw_h, gw_v, lsem.at[12]),
    ]
    ids_own = local(ids_h, idv.at[0], lsem.at[13])
    wc_own = local(
        wc_h.at[:, pl.ds(pl.multiple_of(y * GW, GW), GW)], wc_v.at[y], lsem.at[14]
    )
    kv = kv_v[...]
    keys = kv[:, :HD]
    keys = keys * lax.rsqrt(jnp.mean(keys * keys, axis=-1, keepdims=True) + EPSILON)
    own_slot = (z * NC + c) * OWN
    for i in range(OWN):
        rows = slice(i * PLEN, (i + 1) * PLEN)
        kt_v[own_slot + i] = jnp.transpose(keys[rows]).astype(BF)
        v_v[own_slot + i] = kv[rows, HD:].astype(BF)

    pl.semaphore_wait(barrier, len(partners))
    bufs = (kt_v, v_v)

    last = (((0, 0), (0, 1), (1, 0)), ((0, 2), (1, 1), (1, 2)))

    def core_at(hops):
        return c if hops % 2 == 0 else 1 - c

    def z_copy(d, item, sending):
        kind, k, i = item
        sign = 1 if d == 0 else -1
        hops = k if sending else k + 1
        origin = lax.rem(z - sign * hops + NZ, NZ)
        block = bufs[kind].at[(origin * NC + core_at(hops)) * OWN + i]
        n = ((d * 2 + kind) * 4 + k) * OWN + i
        return remote(block, block, ss.at[0], zr.at[n], dev(dz=sign, other=True))

    def core_copy(kind, o):
        block = bufs[kind].at[pl.ds((lax.rem(z + o, NZ) * NC + core_at(o)) * OWN, OWN)]
        return remote(block, block, ss.at[0], cr.at[kind], dev(other=True))

    def core_send(kind, o):
        core_copy(kind, o).start()

    arrived = set()

    def z_wait(d, item):
        if (d, item) in arrived:
            return
        arrived.add((d, item))
        z_copy(d, item, False).wait_recv()
        kind, k, _ = item
        if k < 3:
            if all((d, (kind, k, i)) in arrived for i in range(OWN)):
                core_send(kind, k + 1 if d == 1 else NZ - k - 1)
        elif all(
            (dd, (kind, 3, i)) in arrived for dd in (0, 1) for kk, i in last[dd] if kk == kind
        ):
            core_send(kind, 4)

    def z_step(n):
        for d in (0, 1):
            item = Z_ORDER[d][n]
            kind, k, i = item
            if k:
                z_wait(d, (kind, k - 1, i))
            cp = z_copy(d, item, True)
            cp.start()

    def z_finish(kind):
        for k in (2, 3):
            for d in (0, 1):
                for i in range(OWN):
                    if k == 2 or (kind, i) in last[d]:
                        z_wait(d, (kind, k, i))

    def core_finish(kind):
        landed(bufs[kind].at[pl.ds(0, NZ * OWN)], cr.at[kind])

    for n in range(5):
        z_step(n)
    for kind in (0, 1):
        core_send(kind, 0)

    for r in (1, 2, 3):
        cp = remote(ids_h, idv.at[NX - r], ids_ss.at[0], ids_rs.at[0], dev(dx=r))
        cp.start()
    for r in (1, 2, 3):
        column = pl.multiple_of(lax.rem(y + r, NY) * GW, GW)
        cp = remote(
            wc_h.at[:, pl.ds(column, GW)], wc_v.at[y], ss.at[0], wcr.at[0], dev(dy=r)
        )
        cp.start()

    gain_load.wait()
    landed(wqp_v, lsem.at[9])
    gain = gain_v[...].reshape(1, D)

    def q_copy(d, m, sending):
        sign = 1 if d == 0 else -1
        if m < 2:
            half, back = m, 0
        else:
            half, back = d, 1
        origin = back if sending else back + 1
        row = (origin if d == 1 else NX - origin) % NX
        at = qg_v.at[row, pl.ds(half * (ROWS // 2), ROWS // 2)]
        back_there = back + 1
        row_there = (back_there if d == 1 else NX - back_there) % NX
        to = qg_v.at[row_there, pl.ds(half * (ROWS // 2), ROWS // 2)] if sending else at
        i = d * 3 + m
        return remote(at, to, ss.at[0], qr.at[i], dev(dx=sign))

    def q_send(d, m):
        cp = q_copy(d, m, True)
        cp.start()

    def token_piece(i):
        tok_loads[i].wait()
        rows = pl.ds(i // 2 * TCHUNK, TCHUNK)
        half = slice(i % 2 * (D // 2), (i % 2 + 1) * (D // 2))
        t = tok_v[rows, half]
        tf = t.astype(F32)
        squares = tf * tf
        folded = squares[:, :128]
        for n in range(1, D // 2 // 128):
            folded = folded + squares[:, n * 128 : (n + 1) * 128]
        term = jnp.dot(t * gain[:, half], wqp_v[half, :], preferred_element_type=F32)
        if i % 2 == 0:
            sq_v[...] = folded
            acc_v[...] = term
            return
        mean = jnp.sum(folded + sq_v[...], axis=-1, keepdims=True) * (1.0 / D)
        both = (term + acc_v[...]) * lax.rsqrt(mean + EPSILON)
        q = both[:, :HD]
        q = q * lax.rsqrt(jnp.mean(q * q, axis=-1, keepdims=True) + EPSILON)
        qg_v[0, rows, :] = q.astype(BF)
        pooled_v[rows, :] = both[:, HD:].astype(BF)

    for i in range(4):
        token_piece(i)
    for d in (0, 1):
        q_send(d, 0)
    z_step(5)
    z_step(6)
    token_piece(4)
    z_step(7)
    z_step(8)
    token_piece(5)
    z_step(9)
    token_piece(6)
    z_step(10)
    z_step(11)
    token_piece(7)
    for d in (0, 1):
        q_send(d, 1)
    z_step(12)
    ids_own.wait()
    landed(idv.at[pl.ds(0, NX - 1)], ids_rs.at[0])
    p = idv[...]
    owner = lax.shift_right_logical(p * 171, 9)
    place = lax.shift_right_logical(owner, 3) * NC + (owner & 1)
    tbl_v[0] = place * OWN + (p - owner * OWN)
    tbl_v[1] = jnp.where((lax.shift_right_logical(owner, 1) & 3) == x, 1, 0)
    tbl_load = local(tbl_v, tbl_s, lsem.at[15])
    for n in (13, 14):
        z_step(n)
    for n in (15, 16):
        z_step(n)
    tbl_load.wait()
    q_copy(0, 0, False).wait_recv()
    q_send(0, 2)
    z_step(17)
    z_finish(0)
    q_copy(1, 1, False).wait_recv()
    q_send(1, 2)
    core_finish(0)
    scale = hs_s[y] * (math.log2(math.e) / math.sqrt(HD))
    row_id = lax.broadcasted_iota(jnp.int32, (SEQ, SEQ), 0)
    col_id = lax.broadcasted_iota(jnp.int32, (SEQ, SEQ), 1)
    eye = row_id == col_id

    def slot_of(r, b, j):
        return tbl_s[0, r, j, b], tbl_s[1, r, j, b] == 1

    none = jnp.zeros((BLOCK, HD), BF)

    def score_pair(r, pair):
        b = (pair * 2, pair * 2 + 1)
        found = [[slot_of(r, n, j) for j in range(NPB)] for n in b]
        q = [qg_v[r, pl.ds(n * BLOCK, BLOCK), :] for n in b]
        left = jnp.concatenate(
            [jnp.concatenate([q[0], none], axis=1), jnp.concatenate([none, q[1]], axis=1)], axis=0
        )
        kt = jnp.concatenate(
            [jnp.concatenate([kt_v[slot] for slot, _ in f], axis=1) for f in found], axis=0
        )
        e = jnp.exp2(jnp.dot(left, kt, preferred_element_type=F32) * scale)
        totals = []
        for u in (0, 1):
            rows = slice(u * BLOCK, (u + 1) * BLOCK)
            es = [
                jnp.where(found[u][j][1], e[rows, j * PLEN : (j + 1) * PLEN], 0.0)
                for j in range(NPB)
            ]
            for j in range(NPB):
                e_v[r, pl.ds(b[u] * BLOCK, BLOCK), pl.ds(j * PLEN, PLEN)] = es[j].astype(BF)
            both = (es[0] + es[1]) + (es[2] + es[3])
            totals.append(jnp.sum(both, axis=1, keepdims=True))
        column = jnp.concatenate(totals, axis=0)
        row = jnp.sum(jnp.where(eye, column, 0.0), axis=0, keepdims=True)
        tot_v[r, pair : pair + 1, :] = row

    def score_group(r, half):
        for u in range(NBLK // 4):
            score_pair(r, half * (NBLK // 4) + u)
        if r and half:
            remote(tot_v.at[r], totg_v.at[NX - r], ts.at[0], tr.at[0], dev(dx=r)).start()

    score_group(0, 0)
    z_step(18)
    score_group(0, 1)
    z_step(19)
    q_copy(1, 0, False).wait_recv()
    score_group(1, 0)
    z_step(20)
    score_group(1, 1)
    q_copy(0, 1, False).wait_recv()
    score_group(3, 0)
    score_group(3, 1)
    for d in (0, 1):
        q_copy(d, 2, False).wait_recv()
    score_group(2, 0)
    z_finish(1)
    score_group(2, 1)
    core_finish(1)

    def step_rows(d, i):
        return pl.ds(d * (ROWS // 2) + i * STEP, STEP)

    def values(pairs):
        for r, d, i in pairs:
            b = d * (NBLK // 2) + i * (STEP // BLOCK)
            rows = pl.ds(b * BLOCK, STEP)
            vv = jnp.concatenate(
                [
                    jnp.concatenate([v_v[slot_of(r, b + u, j)[0]] for j in range(NPB)], axis=0)
                    for u in (0, 1)
                ],
                axis=1,
            )
            o = jnp.dot(e_v[r, rows, :], vv, preferred_element_type=F32)
            part_v[r, pl.ds(b * BLOCK, BLOCK), :] = o[:BLOCK, :HD].astype(BF)
            part_v[r, pl.ds((b + 1) * BLOCK, BLOCK), :] = o[BLOCK:, HD:].astype(BF)

    def r_copy(d, m, i, src, dst):
        n = i if m == 0 else 4 + i
        return remote(src, dst, ss.at[0], rr.at[n], dev(dx=1 if d == 0 else -1))

    def r_send(d, m, i, src, dst):
        cp = r_copy(d, m, i, src, dst)
        cp.start()

    near = (1, 3)

    def far(i):
        values([(2, 0, i), (2, 1, i)])
        for d in (0, 1):
            here = pl.ds(i * STEP, STEP)
            r_send(d, 0, i, part_v.at[2, step_rows(d, i)], rly_v.at[d, here])

    def direct(i):
        values([(near[0], 1, i), (near[1], 0, i)])
        for d in (0, 1):
            rows = step_rows(1 - d, i)
            r_send(d, 1, i, part_v.at[near[d], rows], rrecv_v.at[d, rows])

    def relayed(i):
        values([(near[0], 0, i), (near[1], 1, i)])

    def own(i):
        values([(0, 0, i), (0, 1, i)])

    def relay(i):
        landed(rly_v.at[:, pl.ds(0, STEP)], rr.at[i])
        for d in (0, 1):
            rows = step_rows(d, i)
            here = pl.ds(i * STEP, STEP)
            both = rly_v[d, here, :].astype(F32) + part_v[near[d], rows, :].astype(F32)
            sum_v[d, here, :] = both.astype(BF)
            r_send(d, 2, i, sum_v.at[d, here], rrecv_v.at[d, rows])

    def y_copy(d, m, half, i, sending):
        sign = 1 if d == 0 else -1
        back = (0 if m < 2 else 1) + (0 if sending else 1)
        head = lax.rem(y - sign * back + NY, NY)
        block = att_v.at[head, step_rows(half, i)]
        n = i if m == d else 4 + i
        return remote(block, block, ss.at[0], yr.at[n], dev(dy=sign))

    def y_send(d, m, half, i):
        cp = y_copy(d, m, half, i, True)
        cp.start()

    def attend(i):
        landed(rrecv_v.at[0, pl.ds(0, 4 * STEP)], rr.at[4 + i])
        for half in (0, 1):
            rows = step_rows(half, i)
            pair = half * 4 + i
            row = tot_v[0, pair : pair + 1, :]
            for r in (1, 2, 3):
                row = row + totg_v[r, pair : pair + 1, :]
            total = jnp.sum(jnp.where(eye, row, 0.0), axis=1, keepdims=True)
            summed = (
                part_v[0, rows, :].astype(F32)
                + rrecv_v[0, rows, :].astype(F32)
                + rrecv_v[1, rows, :].astype(F32)
            )
            att_v[y, rows, :] = (summed * (1.0 / total)).astype(BF)
            for d in (0, 1):
                y_send(d, half, half, i)

    def y_forward(i):
        landed(att_v.at[0, pl.ds(0, 2 * STEP)], yr.at[i])
        for d in (0, 1):
            y_send(d, 2, d, i)

    far(0)
    far(1)
    direct(0)
    relayed(0)
    far(2)
    relay(0)
    direct(1)
    relayed(1)
    far(3)
    relay(1)
    direct(2)
    relayed(2)
    own(0)
    relay(2)
    direct(3)
    relayed(3)
    own(1)
    landed(totg_v.at[pl.ds(1, NX - 1)], tr.at[0])
    attend(0)
    relay(3)
    own(2)
    own(3)
    for load in pool_loads:
        load.wait()
    window = lax.shift_left(jnp.int32(2), y.astype(jnp.int32))
    band = jnp.where((col_id <= row_id) & (col_id > row_id - window), 1.0, 0.0).astype(BF)
    position = lax.broadcasted_iota(jnp.int32, (SEQ, GW), 0)
    inverse = 1.0 / jnp.minimum(position + 1, window).astype(F32)
    ps_all = ps_v[...].astype(F32).reshape(1, NY * GW)
    gw_all = gw_v[...].reshape(1, NY * GW)
    ps = jnp.zeros((1, GW), F32)
    gw = jnp.zeros((1, GW), F32)
    for g in range(NY):
        here = y == g
        ps = ps + jnp.where(here, ps_all[:, g * GW : (g + 1) * GW], 0.0)
        gw = gw + jnp.where(here, gw_all[:, g * GW : (g + 1) * GW], 0.0)

    def pool_step(i):
        rows = pl.ds(i * SEQ, SEQ)
        p = pooled_v[rows, :]
        pf = p.astype(F32)
        sums = jnp.dot(band, p, preferred_element_type=F32)
        residual = (sums * inverse - pf).astype(BF)
        pool_v[rows, :] = jnp.dot(residual, wm_v[...], preferred_element_type=F32) * ps
        gate_v[rows, :] = 1.0 / (1.0 + jnp.exp(-(pf * gw)))

    pool_step(0)
    pool_step(4)
    attend(1)
    pool_step(1)
    pool_step(5)
    attend(2)
    y_forward(0)
    attend(3)
    y_forward(1)
    pool_step(2)
    pool_step(6)
    y_forward(2)
    pool_step(3)
    pool_step(7)
    wc_own.wait()
    landed(wc_v.at[pl.ds(0, NY - 1)], wcr.at[0])
    wc = wc_v[...].reshape(NY * HD, GW)

    def cross(i):
        landed(att_v.at[0, pl.ds(0, 4 * STEP)], yr.at[4 + i])
        for half in (0, 1):
            rows = step_rows(half, i)
            att = jnp.concatenate([att_v[h, rows, :] for h in range(NY)], axis=1)
            term = jnp.dot(att, wc, preferred_element_type=F32)
            mixed = pool_v[rows, :] + gate_v[rows, :] * term
            out_v[rows, :] = mixed.astype(BF)
            local(out_v.at[rows], out_h.at[rows], osem.at[0])

    cross(0)
    y_forward(3)
    cross(1)
    cross(2)
    cross(3)
    landed(idv.at[pl.ds(0, NX - 1)], ids_ss.at[0])
    landed(tot_v.at[pl.ds(0, NX - 1)], ts.at[0])
    landed(tok_v.at[pl.ds(0, SENT_ROWS)], ss.at[0])
    landed(out_v, osem.at[0])


def per_device(
    tokens, passage_ids, store, mix_gain, w_query, w_key, w_value, w_cross_out,
    head_scale, w_pool_in, w_pool_mix, pool_scale, gate_weight,
):
    anywhere = pl.BlockSpec(memory_space=pl.ANY)
    dma = pltpu.SemaphoreType.DMA
    in_specs = [anywhere] * 13
    in_specs[8] = pl.BlockSpec(memory_space=pltpu.SMEM)
    v = pltpu.VMEM
    return pl.pallas_call(
        kernel,
        out_shape=jax.ShapeDtypeStruct((ROWS, GW), BF),
        in_specs=in_specs,
        out_specs=anywhere,
        scratch_shapes=[
            v((ROWS, D), BF),
            v((OWN, PLEN, D), BF),
            v((D, 2 * HD), BF),
            v((D, HD + GW), BF),
            v((OWN * PLEN, 2 * HD), F32),
            v((TCHUNK, HD + GW), F32),
            v((TCHUNK, 128), F32),
            v((GW, GW), BF),
            v((D,), BF),
            v((NY * GW,), BF),
            v((NY * GW,), F32),
            v((SLOTS, HD, PLEN), BF),
            v((SLOTS, PLEN, HD), BF),
            v((NX, ROWS, HD), BF),
            v((NX, NPB, NBLK), jnp.int32),
            v((2, NX, NPB, NBLK), jnp.int32),
            pltpu.SMEM((2, NX, NPB, NBLK), jnp.int32),
            v((NY, HD, GW), BF),
            v((ROWS, GW), BF),
            v((ROWS, GW), F32),
            v((ROWS, GW), F32),
            v((NX, ROWS, NPB * PLEN), BF),
            v((NX, ROWS, HD), BF),
            v((2, ROWS // 2, HD), BF),
            v((2, ROWS // 2, HD), BF),
            v((2, ROWS, HD), BF),
            v((NX, 8, 128), F32),
            v((NX, 8, 128), F32),
            v((NY, ROWS, HD), BF),
            v((ROWS, GW), BF),
            dma((16,)),
            dma((PIECES,)),
            dma((1,)),
            dma((1,)),
            dma((48,)),
            dma((2,)),
            dma((6,)),
            dma((1,)), dma((1,)),
            dma((1,)),
            dma((1,)), dma((1,)),
            dma((8,)),
            dma((8,)),
        ],
        compiler_params=pltpu.CompilerParams(
            collective_id=0, has_side_effects=True, vmem_limit_bytes=60 * 1024 * 1024
        ),
        name="mixer",
    )(
        tokens, passage_ids.T, store, mix_gain, w_query, w_key, w_value, w_cross_out,
        head_scale, w_pool_in, w_pool_mix, pool_scale, gate_weight,
    )


def solution(mesh):
    return jax.shard_map(
        per_device,
        mesh=mesh,
        in_specs=(
            P("st", None),
            P("st", None),
            P("st", None, None),
            P(),
            P(None, "tp"),
            P(None, "tp"),
            P(None, "tp"),
            P("tp", None),
            P(),
            P(None, "tp"),
            P(),
            P(),
            P(),
        ),
        out_specs=P("st", "tp"),
        check_vma=False,
    )
```

time: 61.6 us -> 57.4 us (0.932)
  Pallas kernels: 59.6 us -> 55.4 us
    pallas_call x1, Pallas kernels: 59.6 us -> 55.4 us  [per_device(): pl.pallas_call(kernel, out_shape=jax.ShapeDtypeStruct((ROWS, GW), BF), in...]
where the time goes in v3:
time: 57.4 us; the launch traced here: 57.3 us
  Pallas kernels  55.4 us (97%)
  local copies, waits for them, and re-layouts  1.87 us (3%)
    pallas_call x1, Pallas kernels, per_device(): pl.pallas_call(kernel, out_shape=jax.ShapeDtypeStruct((ROWS, GW), BF), in...  55.4 us
    unnamed x1, local copies, waits for them, and re-layouts  1.87 us

profile of v3, /device:TPU:8, one launch (start us, length us, event | category | flops | bytes accessed | tf_op | source)
XLA Modules:
  0.0 57.3 jit_solution(6293503424614664398)
XLA Ops:
  0.0 55.4 %mixer.1 = bf16[1024,256]{1,0:T(8,128)(2,1)} custom-call(bf16[1024,4096]{1,0:T(8,128)(2,1)} %tok_h.1, s32[4,16]{1,0:T(4,128)} %bitcast.1, bf16[3,128,4096]{2,1,0:T(8,128)(2,1)} %store_h.1, bf16[4096]{0:T(1024)(128)(2,1)} %gain_h.1, bf16[4096,128]{1,0:T(8,128)(2,1)} %wq_h.1, bf16[4096,128]{1,0:T(8,128)(2,1)} %wk_h.1, bf16[4096,128]{1,0:T(8,128)(2,1)} %wv_h.1, ...), custom_call_target="tpu_custom_call" | custom-call | tf_op jit(solution)/shard_map/mixer/pallas_call | solution.py:537
  55.4 1.9 %copy.15 = bf16[1024,256]{1,0:T(8,128)(2,1)} copy(bf16[1024,256]{1,0:T(8,128)(2,1)} %mixer.1) | data formatting | bytes 1048576

commit v4 on v3

--- a/solution.py
+++ b/solution.py
@@ -46,11 +46,11 @@
 
 def kernel(
     tok_h, ids_h, store_h, gain_h, wq_h, wk_h, wv_h, wc_h, hs_s, wp_h, wm_h, ps_h, gw_h,
-    out_h,
+    out_v,
     tok_v, store_v, wkv_v, wqp_v, kv_v, acc_v, sq_v, wm_v, gain_v, ps_v, gw_v,
     kt_v, v_v, qg_v, idv, tbl_v, tbl_s, wc_v,
-    pooled_v, pool_v, gate_v, e_v, part_v, rly_v, sum_v, rrecv_v, tot_v, totg_v, att_v, out_v,
-    lsem, tsem, osem,
+    pooled_v, pool_v, gate_v, e_v, part_v, rly_v, sum_v, rrecv_v, tot_v, totg_v, att_v,
+    lsem, tsem,
     ss, zr, cr, qr, ids_ss, ids_rs, wcr, ts, tr, rr, yr,
 ):
     s = lax.axis_index("st")
@@ -105,16 +105,22 @@
         kv_v[...] = term if h == 0 else kv_v[...] + term
 
     kv_part(0)
-    kv_part(1)
-    kv_part(2)
-    kv_part(3)
     gain_load = local(gain_h, gain_v, lsem.at[8])
     local(wq_h, wqp_v.at[:, pl.ds(0, HD)], lsem.at[9])
     local(wp_h, wqp_v.at[:, pl.ds(HD, GW)], lsem.at[9])
     tok_loads = []
-    for i in range(PIECES):
+
+    def load_tokens(i):
         part = (pl.ds(i // 2 * TCHUNK, TCHUNK), pl.ds(i % 2 * (D // 2), D // 2))
         tok_loads.append(local(tok_h.at[part], tok_v.at[part], tsem.at[i]))
+
+    for i in range(4):
+        load_tokens(i)
+    kv_part(1)
+    kv_part(2)
+    kv_part(3)
+    for i in range(4, PIECES):
+        load_tokens(i)
     pool_loads = [
         local(wm_h.at[y], wm_v, lsem.at[10]),
         local(ps_h, ps_v, lsem.at[11]),
@@ -211,24 +217,32 @@
     landed(wqp_v, lsem.at[9])
     gain = gain_v[...].reshape(1, D)
 
-    def q_copy(d, m, sending):
+    def q_copy(d, chunk, back):
         sign = 1 if d == 0 else -1
-        if m < 2:
-            half, back = m, 0
+        rows = pl.ds(chunk * TCHUNK, TCHUNK)
+        here = (-sign * back) % NX
+        there = (-sign * (back + 1)) % NX
+        if back:
+            n = 3
+        elif chunk % 2 == d:
+            n = chunk // 2
         else:
-            half, back = d, 1
-        origin = back if sending else back + 1
-        row = (origin if d == 1 else NX - origin) % NX
-        at = qg_v.at[row, pl.ds(half * (ROWS // 2), ROWS // 2)]
-        back_there = back + 1
-        row_there = (back_there if d == 1 else NX - back_there) % NX
-        to = qg_v.at[row_there, pl.ds(half * (ROWS // 2), ROWS // 2)] if sending else at
-        i = d * 3 + m
-        return remote(at, to, ss.at[0], qr.at[i], dev(dx=sign))
-
-    def q_send(d, m):
-        cp = q_copy(d, m, True)
-        cp.start()
+            n = 2
+        return remote(
+            qg_v.at[here, rows], qg_v.at[there, rows], ss.at[0], qr.at[d * 4 + n], dev(dx=sign)
+        )
+
+    def q_send(chunk):
+        for d in (0, 1):
+            q_copy(d, chunk, 0).start()
+
+    def q_forward(chunk):
+        d = chunk % 2
+        landed(qg_v.at[0, pl.ds(0, TCHUNK)], qr.at[d * 4 + chunk // 2])
+        q_copy(d, chunk, 1).start()
+
+    def q_pair(d, n):
+        landed(qg_v.at[0, pl.ds(0, 2 * TCHUNK)], qr.at[d * 4 + n])
 
     def token_piece(i):
         tok_loads[i].wait()
@@ -252,24 +266,26 @@
         qg_v[0, rows, :] = q.astype(BF)
         pooled_v[rows, :] = both[:, HD:].astype(BF)
 
-    for i in range(4):
-        token_piece(i)
-    for d in (0, 1):
-        q_send(d, 0)
+    token_piece(0)
+    token_piece(1)
+    q_send(0)
     z_step(5)
     z_step(6)
-    token_piece(4)
+    token_piece(2)
     z_step(7)
     z_step(8)
+    token_piece(3)
+    q_send(1)
+    token_piece(4)
+    z_step(9)
+    z_step(10)
     token_piece(5)
-    z_step(9)
+    q_send(2)
+    z_step(11)
+    z_step(12)
     token_piece(6)
-    z_step(10)
-    z_step(11)
     token_piece(7)
-    for d in (0, 1):
-        q_send(d, 1)
-    z_step(12)
+    q_send(3)
     ids_own.wait()
     landed(idv.at[pl.ds(0, NX - 1)], ids_rs.at[0])
     p = idv[...]
@@ -283,12 +299,12 @@
     for n in (15, 16):
         z_step(n)
     tbl_load.wait()
-    q_copy(0, 0, False).wait_recv()
-    q_send(0, 2)
+    q_forward(0)
+    q_forward(1)
     z_step(17)
+    q_forward(2)
+    q_forward(3)
     z_finish(0)
-    q_copy(1, 1, False).wait_recv()
-    q_send(1, 2)
     core_finish(0)
     scale = hs_s[y] * (math.log2(math.e) / math.sqrt(HD))
     row_id = lax.broadcasted_iota(jnp.int32, (SEQ, SEQ), 0)
@@ -311,18 +327,25 @@
             [jnp.concatenate([kt_v[slot] for slot, _ in f], axis=1) for f in found], axis=0
         )
         e = jnp.exp2(jnp.dot(left, kt, preferred_element_type=F32) * scale)
-        totals = []
-        for u in (0, 1):
-            rows = slice(u * BLOCK, (u + 1) * BLOCK)
-            es = [
-                jnp.where(found[u][j][1], e[rows, j * PLEN : (j + 1) * PLEN], 0.0)
-                for j in range(NPB)
-            ]
-            for j in range(NPB):
-                e_v[r, pl.ds(b[u] * BLOCK, BLOCK), pl.ds(j * PLEN, PLEN)] = es[j].astype(BF)
-            both = (es[0] + es[1]) + (es[2] + es[3])
-            totals.append(jnp.sum(both, axis=1, keepdims=True))
-        column = jnp.concatenate(totals, axis=0)
+        e = jnp.concatenate(
+            [
+                jnp.concatenate(
+                    [
+                        jnp.where(
+                            found[u][j][1],
+                            e[u * BLOCK : (u + 1) * BLOCK, j * PLEN : (j + 1) * PLEN], 0.0,
+                        )
+                        for j in range(NPB)
+                    ],
+                    axis=1,
+                )
+                for u in (0, 1)
+            ],
+            axis=0,
+        )
+        e_v[r, pl.ds(pair * 2 * BLOCK, 2 * BLOCK), :] = e.astype(BF)
+        es = [e[:, j * PLEN : (j + 1) * PLEN] for j in range(NPB)]
+        column = jnp.sum((es[0] + es[1]) + (es[2] + es[3]), axis=1, keepdims=True)
         row = jnp.sum(jnp.where(eye, column, 0.0), axis=0, keepdims=True)
         tot_v[r, pair : pair + 1, :] = row
 
@@ -336,15 +359,15 @@
     z_step(18)
     score_group(0, 1)
     z_step(19)
-    q_copy(1, 0, False).wait_recv()
+    q_pair(1, 2)
     score_group(1, 0)
     z_step(20)
     score_group(1, 1)
-    q_copy(0, 1, False).wait_recv()
+    q_pair(0, 2)
     score_group(3, 0)
     score_group(3, 1)
     for d in (0, 1):
-        q_copy(d, 2, False).wait_recv()
+        q_pair(d, 3)
     score_group(2, 0)
     z_finish(1)
     score_group(2, 1)
@@ -512,7 +535,6 @@
             term = jnp.dot(att, wc, preferred_element_type=F32)
             mixed = pool_v[rows, :] + gate_v[rows, :] * term
             out_v[rows, :] = mixed.astype(BF)
-            local(out_v.at[rows], out_h.at[rows], osem.at[0])
 
     cross(0)
     y_forward(3)
@@ -522,23 +544,22 @@
     landed(idv.at[pl.ds(0, NX - 1)], ids_ss.at[0])
     landed(tot_v.at[pl.ds(0, NX - 1)], ts.at[0])
     landed(tok_v.at[pl.ds(0, SENT_ROWS)], ss.at[0])
-    landed(out_v, osem.at[0])
 
 
 def per_device(
     tokens, passage_ids, store, mix_gain, w_query, w_key, w_value, w_cross_out,
     head_scale, w_pool_in, w_pool_mix, pool_scale, gate_weight,
 ):
-    anywhere = pl.BlockSpec(memory_space=pl.ANY)
+    in_hbm = pl.BlockSpec(memory_space=pltpu.HBM)
     dma = pltpu.SemaphoreType.DMA
-    in_specs = [anywhere] * 13
+    in_specs = [in_hbm] * 13
     in_specs[8] = pl.BlockSpec(memory_space=pltpu.SMEM)
     v = pltpu.VMEM
     return pl.pallas_call(
         kernel,
         out_shape=jax.ShapeDtypeStruct((ROWS, GW), BF),
         in_specs=in_specs,
-        out_specs=anywhere,
+        out_specs=pl.BlockSpec(memory_space=pltpu.VMEM),
         scratch_shapes=[
             v((ROWS, D), BF),
             v((OWN, PLEN, D), BF),
@@ -569,14 +590,12 @@
             v((NX, 8, 128), F32),
             v((NX, 8, 128), F32),
             v((NY, ROWS, HD), BF),
-            v((ROWS, GW), BF),
             dma((16,)),
             dma((PIECES,)),
             dma((1,)),
-            dma((1,)),
             dma((48,)),
             dma((2,)),
-            dma((6,)),
+            dma((8,)),
             dma((1,)), dma((1,)),
             dma((1,)),
             dma((1,)), dma((1,)),

time: 57.4 us -> 55.7 us (0.970)
  Pallas kernels: 55.4 us -> 53.7 us
    pallas_call x1, Pallas kernels: 55.4 us -> 53.7 us  [per_device(): pl.pallas_call(kernel, out_shape=jax.ShapeDtypeStruct((ROWS, GW), BF), in...]
where the time goes in v4:
time: 55.7 us; the launch traced here: 55.6 us
  Pallas kernels  53.7 us (96%)
  local copies, waits for them, and re-layouts  1.87 us (3%)
    pallas_call x1, Pallas kernels, per_device(): pl.pallas_call(kernel, out_shape=jax.ShapeDtypeStruct((ROWS, GW), BF), in...  53.7 us
    unnamed x1, local copies, waits for them, and re-layouts  1.87 us

profile of v4, /device:TPU:8, one launch (start us, length us, event | category | flops | bytes accessed | tf_op | source)
XLA Modules:
  0.0 55.6 jit_solution(15062132100953034448)
XLA Ops:
  0.0 53.7 %mixer.1 = bf16[1024,256]{1,0:T(8,128)(2,1)} custom-call(bf16[1024,4096]{1,0:T(8,128)(2,1)} %tok_h.1, s32[4,16]{1,0:T(4,128)} %bitcast.1, bf16[3,128,4096]{2,1,0:T(8,128)(2,1)} %store_h.1, bf16[4096]{0:T(1024)(128)(2,1)} %gain_h.1, bf16[4096,128]{1,0:T(8,128)(2,1)} %wq_h.1, bf16[4096,128]{1,0:T(8,128)(2,1)} %wk_h.1, bf16[4096,128]{1,0:T(8,128)(2,1)} %wv_h.1, ...), custom_call_target="tpu_custom_call" | custom-call | tf_op jit(solution)/shard_map/mixer/pallas_call | solution.py:558
  53.7 1.9 %copy.15 = bf16[1024,256]{1,0:T(8,128)(2,1)} copy(bf16[1024,256]{1,0:T(8,128)(2,1)} %mixer.1) | data formatting | bytes 1048576

commit v5 on v4

--- a/solution.py
+++ b/solution.py
@@ -38,8 +38,8 @@
 Z_ORDER = tuple(
     tuple((n // 100, n // 10 % 10, n % 10) for n in codes)
     for codes in (
-        (1, 0, 101, 2, 100, 10, 11, 12, 102, 20, 21, 110, 22, 30, 31, 111, 112, 120, 121, 122, 130),
-        (1, 0, 2, 102, 101, 10, 12, 11, 100, 111, 22, 21, 20, 112, 32, 121, 110, 122, 131, 120, 132),
+        (0, 1, 102, 2, 101, 100, 10, 11, 12, 111, 110, 20, 21, 112, 22, 120, 30, 31, 122, 121, 130),
+        (2, 1, 100, 101, 0, 102, 12, 11, 111, 110, 112, 10, 22, 121, 21, 122, 20, 32, 120, 131, 132),
     )
 )
 
@@ -106,8 +106,6 @@
 
     kv_part(0)
     gain_load = local(gain_h, gain_v, lsem.at[8])
-    local(wq_h, wqp_v.at[:, pl.ds(0, HD)], lsem.at[9])
-    local(wp_h, wqp_v.at[:, pl.ds(HD, GW)], lsem.at[9])
     tok_loads = []
 
     def load_tokens(i):
@@ -115,6 +113,10 @@
         tok_loads.append(local(tok_h.at[part], tok_v.at[part], tsem.at[i]))
 
     for i in range(4):
+        if i < 2:
+            part = pl.ds(i * (D // 2), D // 2)
+            local(wq_h.at[part], wqp_v.at[part, pl.ds(0, HD)], lsem.at[9 if i == 0 else 16])
+            local(wp_h.at[part], wqp_v.at[part, pl.ds(HD, GW)], lsem.at[9 if i == 0 else 16])
         load_tokens(i)
     kv_part(1)
     kv_part(2)
@@ -198,7 +200,7 @@
     def core_finish(kind):
         landed(bufs[kind].at[pl.ds(0, NZ * OWN)], cr.at[kind])
 
-    for n in range(5):
+    for n in range(6):
         z_step(n)
     for kind in (0, 1):
         core_send(kind, 0)
@@ -214,7 +216,6 @@
         cp.start()
 
     gain_load.wait()
-    landed(wqp_v, lsem.at[9])
     gain = gain_v[...].reshape(1, D)
 
     def q_copy(d, chunk, back):
@@ -245,6 +246,8 @@
         landed(qg_v.at[0, pl.ds(0, 2 * TCHUNK)], qr.at[d * 4 + n])
 
     def token_piece(i):
+        if i < 2:
+            landed(wqp_v.at[pl.ds(i * (D // 2), D // 2)], lsem.at[9 if i == 0 else 16])
         tok_loads[i].wait()
         rows = pl.ds(i // 2 * TCHUNK, TCHUNK)
         half = slice(i % 2 * (D // 2), (i % 2 + 1) * (D // 2))
@@ -269,23 +272,25 @@
     token_piece(0)
     token_piece(1)
     q_send(0)
-    z_step(5)
     z_step(6)
+    z_step(7)
     token_piece(2)
-    z_step(7)
-    z_step(8)
     token_piece(3)
     q_send(1)
+    z_step(8)
     token_piece(4)
     z_step(9)
-    z_step(10)
     token_piece(5)
     q_send(2)
+    z_step(10)
     z_step(11)
+    token_piece(6)
     z_step(12)
-    token_piece(6)
     token_piece(7)
     q_send(3)
+    z_step(13)
+    z_step(14)
+    q_forward(0)
     ids_own.wait()
     landed(idv.at[pl.ds(0, NX - 1)], ids_rs.at[0])
     p = idv[...]
@@ -294,17 +299,19 @@
     tbl_v[0] = place * OWN + (p - owner * OWN)
     tbl_v[1] = jnp.where((lax.shift_right_logical(owner, 1) & 3) == x, 1, 0)
     tbl_load = local(tbl_v, tbl_s, lsem.at[15])
-    for n in (13, 14):
-        z_step(n)
-    for n in (15, 16):
-        z_step(n)
+    z_step(15)
+    q_forward(1)
+    z_step(16)
+    q_forward(2)
+    z_step(17)
     tbl_load.wait()
-    q_forward(0)
-    q_forward(1)
-    z_step(17)
-    q_forward(2)
+    z_step(18)
+    z_step(19)
     q_forward(3)
+    z_step(20)
     z_finish(0)
+    q_pair(1, 2)
+    q_pair(0, 2)
     core_finish(0)
     scale = hs_s[y] * (math.log2(math.e) / math.sqrt(HD))
     row_id = lax.broadcasted_iota(jnp.int32, (SEQ, SEQ), 0)
@@ -356,20 +363,15 @@
             remote(tot_v.at[r], totg_v.at[NX - r], ts.at[0], tr.at[0], dev(dx=r)).start()
 
     score_group(0, 0)
-    z_step(18)
     score_group(0, 1)
-    z_step(19)
-    q_pair(1, 2)
     score_group(1, 0)
-    z_step(20)
     score_group(1, 1)
-    q_pair(0, 2)
+    z_finish(1)
+    for d in (0, 1):
+        q_pair(d, 3)
     score_group(3, 0)
     score_group(3, 1)
-    for d in (0, 1):
-        q_pair(d, 3)
     score_group(2, 0)
-    z_finish(1)
     score_group(2, 1)
     core_finish(1)
 
@@ -590,7 +592,7 @@
             v((NX, 8, 128), F32),
             v((NX, 8, 128), F32),
             v((NY, ROWS, HD), BF),
-            dma((16,)),
+            dma((17,)),
             dma((PIECES,)),
             dma((1,)),
             dma((48,)),

time: 55.7 us -> 52.6 us (0.944)
  Pallas kernels: 53.7 us -> 50.6 us
    pallas_call x1, Pallas kernels: 53.7 us -> 50.6 us  [per_device(): pl.pallas_call(kernel, out_shape=jax.ShapeDtypeStruct((ROWS, GW), BF), in...]
where the time goes in v5:
time: 52.6 us; the launch traced here: 52.5 us
  Pallas kernels  50.6 us (96%)
  local copies, waits for them, and re-layouts  1.87 us (4%)
    pallas_call x1, Pallas kernels, per_device(): pl.pallas_call(kernel, out_shape=jax.ShapeDtypeStruct((ROWS, GW), BF), in...  50.6 us
    unnamed x1, local copies, waits for them, and re-layouts  1.87 us

profile of v5, /device:TPU:8, one launch (start us, length us, event | category | flops | bytes accessed | tf_op | source)
XLA Modules:
  0.0 52.5 jit_solution(18379885502936787885)
XLA Ops:
  0.0 50.6 %mixer.1 = bf16[1024,256]{1,0:T(8,128)(2,1)} custom-call(bf16[1024,4096]{1,0:T(8,128)(2,1)} %tok_h.1, s32[4,16]{1,0:T(4,128)} %bitcast.1, bf16[3,128,4096]{2,1,0:T(8,128)(2,1)} %store_h.1, bf16[4096]{0:T(1024)(128)(2,1)} %gain_h.1, bf16[4096,128]{1,0:T(8,128)(2,1)} %wq_h.1, bf16[4096,128]{1,0:T(8,128)(2,1)} %wk_h.1, bf16[4096,128]{1,0:T(8,128)(2,1)} %wv_h.1, ...), custom_call_target="tpu_custom_call" | custom-call | tf_op jit(solution)/shard_map/mixer/pallas_call | solution.py:560
  50.7 1.9 %copy.15 = bf16[1024,256]{1,0:T(8,128)(2,1)} copy(bf16[1024,256]{1,0:T(8,128)(2,1)} %mixer.1) | data formatting | bytes 1048576

commit v6 on v5

--- a/solution.py
+++ b/solution.py
@@ -155,7 +155,8 @@
         hops = k if sending else k + 1
         origin = lax.rem(z - sign * hops + NZ, NZ)
         block = bufs[kind].at[(origin * NC + core_at(hops)) * OWN + i]
-        n = ((d * 2 + kind) * 4 + k) * OWN + i
+        onward = (kind, k + 1, i)
+        n = Z_ORDER[d].index(onward) if onward in Z_ORDER[d] else len(Z_ORDER[d]) + kind
         return remote(block, block, ss.at[0], zr.at[n], dev(dz=sign, other=True))
 
     def core_copy(kind, o):
@@ -167,11 +168,8 @@
 
     arrived = set()
 
-    def z_wait(d, item):
-        if (d, item) in arrived:
-            return
+    def z_arrived(d, item):
         arrived.add((d, item))
-        z_copy(d, item, False).wait_recv()
         kind, k, _ = item
         if k < 3:
             if all((d, (kind, k, i)) in arrived for i in range(OWN)):
@@ -182,20 +180,23 @@
             core_send(kind, 4)
 
     def z_step(n):
+        if n >= 6:
+            landed(kt_v.at[pl.ds(0, 2)], zr.at[n])
         for d in (0, 1):
-            item = Z_ORDER[d][n]
-            kind, k, i = item
+            z_copy(d, Z_ORDER[d][n], True).start()
+        for d in (0, 1):
+            kind, k, i = Z_ORDER[d][n]
             if k:
-                z_wait(d, (kind, k - 1, i))
-            cp = z_copy(d, item, True)
-            cp.start()
+                z_arrived(d, (kind, k - 1, i))
 
     def z_finish(kind):
+        landed(kt_v.at[pl.ds(0, 6)], zr.at[len(Z_ORDER[0]) + kind])
         for k in (2, 3):
             for d in (0, 1):
                 for i in range(OWN):
-                    if k == 2 or (kind, i) in last[d]:
-                        z_wait(d, (kind, k, i))
+                    stays = (kind, i) in last[d] if k == 3 else (kind, i) not in last[d]
+                    if stays:
+                        z_arrived(d, (kind, k, i))
 
     def core_finish(kind):
         landed(bufs[kind].at[pl.ds(0, NZ * OWN)], cr.at[kind])
@@ -457,7 +458,9 @@
                 + rrecv_v[1, rows, :].astype(F32)
             )
             att_v[y, rows, :] = (summed * (1.0 / total)).astype(BF)
+        for first in (0, 1):
             for d in (0, 1):
+                half = d if first == 0 else 1 - d
                 y_send(d, half, half, i)
 
     def y_forward(i):
@@ -595,7 +598,7 @@
             dma((17,)),
             dma((PIECES,)),
             dma((1,)),
-            dma((48,)),
+            dma((23,)),
             dma((2,)),
             dma((8,)),
             dma((1,)), dma((1,)),

time: 52.6 us -> 52.9 us (level)
  no operation moved by 1% of the time
where the time goes in v6:
time: 52.9 us; the launch traced here: 52.7 us
  Pallas kernels  50.9 us (96%)
  local copies, waits for them, and re-layouts  1.87 us (4%)
    pallas_call x1, Pallas kernels, per_device(): pl.pallas_call(kernel, out_shape=jax.ShapeDtypeStruct((ROWS, GW), BF), in...  50.9 us
    unnamed x1, local copies, waits for them, and re-layouts  1.87 us

profile of v6, /device:TPU:8, one launch (start us, length us, event | category | flops | bytes accessed | tf_op | source)
XLA Modules:
  0.0 52.7 jit_solution(6242803937089992749)
XLA Ops:
  0.0 50.9 %mixer.1 = bf16[1024,256]{1,0:T(8,128)(2,1)} custom-call(bf16[1024,4096]{1,0:T(8,128)(2,1)} %tok_h.1, s32[4,16]{1,0:T(4,128)} %bitcast.1, bf16[3,128,4096]{2,1,0:T(8,128)(2,1)} %store_h.1, bf16[4096]{0:T(1024)(128)(2,1)} %gain_h.1, bf16[4096,128]{1,0:T(8,128)(2,1)} %wq_h.1, bf16[4096,128]{1,0:T(8,128)(2,1)} %wk_h.1, bf16[4096,128]{1,0:T(8,128)(2,1)} %wv_h.1, ...), custom_call_target="tpu_custom_call" | custom-call | tf_op jit(solution)/shard_map/mixer/pallas_call | solution.py:563
  50.9 1.9 %copy.15 = bf16[1024,256]{1,0:T(8,128)(2,1)} copy(bf16[1024,256]{1,0:T(8,128)(2,1)} %mixer.1) | data formatting | bytes 1048576
